TPU v7x, 1024 devices: a whole 8x8x8 slice. The times are simulated.
1024 devices in a mesh: fs: 64 (over z, y), tp: 16 (over x, core).
Axes of the slice: x: 8, y: 8, z: 8, core: 2. Of those that a mesh axis runs over, the one named last changes fastest.
Arguments:
- tokens: bfloat16 [24576, 2048], P('fs'), may hold values from -6 to 6
- norm_gain: float32 [2048], replicated, may hold values from 0.1 to 1.9
- w_gate: bfloat16 [2048, 4096], P('fs', 'tp'), may hold values from -0.125 to 0.125
- w_up: bfloat16 [2048, 4096], P('fs', 'tp'), may hold values from -0.125 to 0.125
- w_down: bfloat16 [4096, 2048], P('tp', 'fs'), may hold values from -0.09375 to 0.09375
- cotangent: bfloat16 [24576, 2048], P('fs'), may hold values from -16 to 16
Outputs:
- grad_tokens: bfloat16 [24576, 2048], P('fs')
- grad_down: float32 [4096, 2048], P('tp', 'fs')
- down_norms: float32 [4096], P('tp')
All inputs are finite; a program needn't handle non-finite values.
Results may differ from a plain program's by a relative error of at most 0.018.
Values may be sent and summed in bfloat16 or wider, within the bound.
No kernel may reach another device: no remote copies, remote signals or barrier semaphores. Data moves between devices by JAX's collectives and lax.ppermute only.
A program may use at most 32 MiB of HBM per device.

v0:
```python
import jax
import jax.numpy as jnp
from jax import lax
from jax.sharding import Mesh
from jax.sharding import PartitionSpec as P


FS = ("z", "y")
TP = ("x", "c")


EPS = 1e-06


def swap(pieces, axis):
    return lax.all_to_all(pieces, axis, split_axis=0, concat_axis=0, tiled=True)


def copy_for_each(shard, axis):
    return swap(jnp.broadcast_to(shard, (lax.axis_size(axis), *shard.shape)), axis)


def shift(value, axis, by):
    peers = lax.axis_size(axis)
    return lax.ppermute(value, axis, [(i, (i + by) % peers) for i in range(peers)])


def exchange(value, axis, bit):
    return lax.ppermute(value, axis, [(i, i ^ bit) for i in range(lax.axis_size(axis))])


def after(value, *others):
    return lax.optimization_barrier((value, *others))[0]


def ring(block, axis):
    peers, here = lax.axis_size(axis), lax.axis_index(axis)
    a, b, c = block.shape
    whole = jnp.zeros((a, peers, b, c), block.dtype)

    def put(whole, piece, index):
        return lax.dynamic_update_slice(whole, piece[:, None], (0, index % peers, 0, 0))

    whole = put(whole, block, here)
    forth = back = block
    for step in range(1, peers // 2 + 1):
        forth = shift(forth, axis, 1)
        if step < peers // 2:
            back = shift(back, axis, -1)
            whole = put(whole, back, here + step)
        whole = put(whole, forth, here + peers - step)
    return whole


def shards(tokens, norm_gain, w_gate, w_up, w_down, cotangent):
    f32, bf16 = jnp.float32, jnp.bfloat16
    rows, width = tokens.shape
    part_rows, units = w_gate.shape
    sizes = {a: lax.axis_size(a) for a in ("z", "y", "x", "c")}

    both = copy_for_each(jnp.concatenate([w_gate, w_up], axis=1), "z")
    down = copy_for_each(after(w_down.T, both), "y")
    full_down = copy_for_each(down, "z").reshape(width, units)
    both = ring(both, "y").reshape(width, 2 * units)
    full_gate, full_up = both[:, :units], both[:, units:]

    xf = tokens.astype(f32)
    inv = lax.rsqrt(jnp.mean(xf * xf, axis=-1, keepdims=True) + EPS)
    normed = (xf * inv * norm_gain).astype(bf16)
    gate = jnp.dot(normed, full_gate, preferred_element_type=f32)
    up = jnp.dot(normed, full_up, preferred_element_type=f32)
    sig = jax.nn.sigmoid(gate)
    act = gate * sig
    hidden = (act * up).astype(bf16)

    down_part = 0.5 * lax.dot_general(
        cotangent, hidden, (((0,), (0,)), ((), ())), preferred_element_type=f32
    )
    down_part = down_part.astype(bf16).reshape(-1, part_rows, units)
    down_pieces = swap(down_part, FS)

    full_down = after(full_down, down_part)
    d_hidden = 0.5 * jnp.dot(cotangent, full_down, preferred_element_type=f32)
    d_gate = (d_hidden * up * sig * (1.0 + gate * (1.0 - sig))).astype(bf16)
    d_up = (d_hidden * act).astype(bf16)

    part = lax.dot_general(d_gate, full_gate, (((1,), (1,)), ((), ())), preferred_element_type=f32)
    part = part + lax.dot_general(
        d_up, full_up, (((1,), (1,)), ((), ())), preferred_element_type=f32
    )
    core, place = lax.axis_index("c"), lax.axis_index("x")
    pair = part.astype(bf16).reshape(sizes["c"], rows // sizes["c"], width)
    theirs = lax.dynamic_index_in_dim(pair, 1 - core, 0, False)
    theirs = exchange(theirs, "c", 1)
    mine = lax.dynamic_index_in_dim(pair, core, 0, False)
    own = mine.shape[0] // sizes["x"]

    def piece(index):
        start = (index % sizes["x"]) * own
        return lax.dynamic_slice_in_dim(mine, start, own, 0).astype(
            f32
        ) + lax.dynamic_slice_in_dim(theirs, start, own, 0).astype(f32)

    d_share = piece(place)
    for by in (4, 3, 5, 2, 6, 1, 7):
        d_share = d_share + shift(piece(place + by).astype(bf16), "x", by).astype(f32)
    offset = (core * sizes["x"] + place) * own
    own_tokens = lax.dynamic_slice_in_dim(tokens, offset, own, 0).astype(f32)
    own_inv = lax.rsqrt(jnp.mean(own_tokens * own_tokens, axis=-1, keepdims=True) + EPS)
    scaled = own_tokens * own_inv
    d_scaled = d_share * norm_gain
    inner = jnp.mean(d_scaled * scaled, axis=-1, keepdims=True)
    grad_own = (own_inv * (d_scaled - scaled * inner)).astype(bf16)
    share = jnp.sum(down_pieces.astype(f32), axis=0)
    norms = jnp.sum(share * share, axis=0)
    norms = copy_for_each(norms, FS)
    grad_half = ring(grad_own[None], "x").reshape(1, -1, width)
    others = exchange(grad_half, "c", 1)
    grad_tokens = jnp.zeros((sizes["c"], *grad_half.shape[1:]), bf16)
    grad_tokens = lax.dynamic_update_slice(grad_tokens, grad_half, (core, 0, 0))
    grad_tokens = lax.dynamic_update_slice(grad_tokens, others, (1 - core, 0, 0))
    grad_tokens = grad_tokens.reshape(rows, width)
    return (grad_tokens, share.T, jnp.sum(norms, axis=0))


def solution(mesh):
    split = Mesh(mesh.devices.reshape(8, 8, 8, 2), ("z", "y", "x", "c"))
    placed = (P(FS, None), P(), P(FS, TP), P(FS, TP), P(TP, FS), P(FS, None))
    return jax.shard_map(
        shards,
        mesh=split,
        in_specs=placed,
        out_specs=(P(FS, None), P(TP, FS), P(TP)),
        check_vma=False,
    )
```

profile of v0, /device:TPU:1, one launch (start us, length us, event | category | flops | bytes accessed | tf_op | source)
XLA Modules:
  0.0 226.9 jit_solution(2120437979280989350)
XLA Ops:
  0.7 0.9 pad_maximum_fusion
  1.5 0.7 broadcast_in_dim.76
  2.2 17.2 %all-to-all-start = ((bf16[8,32,512]{2,1,0:T(8,128)(2,1)}), bf16[8,32,512]{2,1,0:T(8,128)(2,1)S(1)}, u32[]{:S(2)}, u32[]{:S(2)}) async-start(bf16[8,32,512]{2,1,0:T(8,128)(2,1)} %broadcast_in_dim.76), calls=%async_computation | async-start | bytes 524288 | tf_op jit(solution)/shard_map/all_to_all | solution.py:16
  19.5 1.8 fusion
  21.3 8.7 %all-to-all-done = bf16[8,32,512]{2,1,0:T(8,128)(2,1)S(1)} async-done(((bf16[8,32,512]{2,1,0:T(8,128)(2,1)}), bf16[8,32,512]{2,1,0:T(8,128)(2,1)S(1)}, u32[]{:S(2)}, u32[]{:S(2)}) %all-to-all-start) | async-done | bytes 262176 | tf_op jit(solution)/shard_map/all_to_all | solution.py:16
  30.0 5.9 %collective-permute-start = (bf16[8,32,512]{2,1,0:T(8,128)(2,1)S(1)}, bf16[8,32,512]{2,1,0:T(8,128)(2,1)S(1)}, u32[]{:S(2)}, u32[]{:S(2)}) collective-permute-start(bf16[8,32,512]{2,1,0:T(8,128)(2,1)S(1)} %all-to-all-done), channel_id=1, source_target_pairs={{0,112},{16,0},{32,16},{48,32},{64,48},{80,64},{96,80},{112,96},{1... | collective-permute-start | bytes 786440 | tf_op jit(solution)/shard_map/ppermute | solution.py:25
  35.9 1.9 collective-permute-start.1
  38.6 4.7 %all-to-all-start.1 = ((bf16[8,32,256]{2,1,0:T(8,128)(2,1)}), bf16[8,32,256]{2,1,0:T(8,128)(2,1)S(1)}, u32[]{:S(2)}, u32[]{:S(2)}) async-start(bf16[8,32,256]{2,1,0:T(8,128)(2,1)} %broadcast_in_dim.77), calls=%async_computation.1 | async-start | bytes 262144 | tf_op jit(solution)/shard_map/all_to_all | solution.py:16
  43.3 1.6 broadcast_in_dim.79
  44.9 0.7 bitcast_dynamic-update-slice_fusion.6
  45.7 5.7 %all-to-all-done.1 = bf16[8,32,256]{2,1,0:T(8,128)(2,1)S(1)} async-done(((bf16[8,32,256]{2,1,0:T(8,128)(2,1)}), bf16[8,32,256]{2,1,0:T(8,128)(2,1)S(1)}, u32[]{:S(2)}, u32[]{:S(2)}) %all-to-all-start.1) | async-done | bytes 131104 | tf_op jit(solution)/shard_map/all_to_all | solution.py:16
  51.4 1.1 broadcast_in_dim.78
  52.5 4.2 %all-to-all-start.2 = ((bf16[8,8,32,256]{3,2,1,0:T(8,128)(2,1)}), bf16[8,8,32,256]{3,2,1,0:T(8,128)(2,1)}, u32[]{:S(2)}, u32[]{:S(2)}) async-start(bf16[8,8,32,256]{3,2,1,0:T(8,128)(2,1)} %broadcast_in_dim.78), calls=%async_computation.2 | async-start | bytes 2097152 | tf_op jit(solution)/shard_map/all_to_all | solution.py:16
  56.7 2.1 collective-permute-start.2
  58.8 3.4 %collective-permute-start.3 = (bf16[8,32,512]{2,1,0:T(8,128)(2,1)S(1)}, bf16[8,32,512]{2,1,0:T(8,128)(2,1)S(1)}, u32[]{:S(2)}, u32[]{:S(2)}) collective-permute-start(bf16[8,32,512]{2,1,0:T(8,128)(2,1)S(1)} %collective-permute-done.1), channel_id=1, source_target_pairs={{0,16},{16,32},{32,48},{48,64},{64,80},{80,96},{96,112},{112,0},{1... | collective-permute-start | bytes 786440 | tf_op jit(solution)/shard_map/ppermute | solution.py:25
  62.2 0.8 bitcast_dynamic-update-slice_fusion.5
  62.9 0.8 bitcast_dynamic-update-slice_fusion.4
  64.4 2.7 %collective-permute-start.4 = (bf16[8,32,512]{2,1,0:T(8,128)(2,1)S(1)}, bf16[8,32,512]{2,1,0:T(8,128)(2,1)S(1)}, u32[]{:S(2)}, u32[]{:S(2)}) collective-permute-start(bf16[8,32,512]{2,1,0:T(8,128)(2,1)S(1)} %collective-permute-done.2), channel_id=1, source_target_pairs={{0,112},{16,0},{32,16},{48,32},{64,48},{80,64},{96,80},{112,96},{1... | collective-permute-start | bytes 786440 | tf_op jit(solution)/shard_map/ppermute | solution.py:25
  67.1 2.5 %collective-permute-start.5 = (bf16[8,32,512]{2,1,0:T(8,128)(2,1)S(1)}, bf16[8,32,512]{2,1,0:T(8,128)(2,1)S(1)}, u32[]{:S(2)}, u32[]{:S(2)}) collective-permute-start(bf16[8,32,512]{2,1,0:T(8,128)(2,1)S(1)} %collective-permute-done.3), channel_id=1, source_target_pairs={{0,16},{16,32},{32,48},{48,64},{64,80},{80,96},{96,112},{112,0},{1... | collective-permute-start | bytes 786440 | tf_op jit(solution)/shard_map/ppermute | solution.py:25
  69.7 0.8 bitcast_dynamic-update-slice_fusion.3
  70.4 0.8 bitcast_dynamic-update-slice_fusion.2
  71.2 4.6 %collective-permute-done.5 = bf16[8,32,512]{2,1,0:T(8,128)(2,1)S(1)} collective-permute-done((bf16[8,32,512]{2,1,0:T(8,128)(2,1)S(1)}, bf16[8,32,512]{2,1,0:T(8,128)(2,1)S(1)}, u32[]{:S(2)}, u32[]{:S(2)}) %collective-permute-start.5) | collective-permute-done | bytes 262176 | tf_op jit(solution)/shard_map/ppermute | solution.py:25
  75.9 1.9 collective-permute-start.6
  77.8 0.8 bitcast_dynamic-update-slice_fusion.1
  79.3 5.3 %collective-permute-done.6 = bf16[8,32,512]{2,1,0:T(8,128)(2,1)S(1)} collective-permute-done((bf16[8,32,512]{2,1,0:T(8,128)(2,1)S(1)}, bf16[8,32,512]{2,1,0:T(8,128)(2,1)S(1)}, u32[]{:S(2)}, u32[]{:S(2)}) %collective-permute-start.6) | collective-permute-done | bytes 262176 | tf_op jit(solution)/shard_map/ppermute | solution.py:25
  84.6 0.8 bitcast_dynamic-update-slice_fusion.7
  85.3 1.8 fusion.11
  87.2 1.8 fusion.8
  89.1 0.8 fusion.4
  89.8 1.3 copy.35
  91.1 1.8 fusion.5
  93.0 1.9 fusion.6
  94.9 1.9 add_convert_fusion
  96.8 0.9 dynamic-slice_bitcast_fusion
  97.7 8.8 %collective-permute-start.7 = (bf16[192,2048]{1,0:T(8,128)(2,1)}, bf16[192,2048]{1,0:T(8,128)(2,1)}, u32[]{:S(2)}, u32[]{:S(2)}) collective-permute-start(bf16[192,2048]{1,0:T(8,128)(2,1)} %dynamic-slice_bitcast_fusion), channel_id=1, source_target_pairs={{0,1},{1,0},{2,3},{3,2},{4,5},{5,4},{6,7},{7,6},{8,9},{9,8},{10,11... | collective-permute-start | bytes 2359304 | tf_op jit(solution)/shard_map/ppermute | solution.py:29
  106.7 2.1 collective-permute-done.7
  108.8 2.1 fusion.29
  110.9 6.2 %collective-permute-start.10 = (bf16[24,2048]{1,0:T(8,128)(2,1)}, bf16[24,2048]{1,0:T(8,128)(2,1)}, u32[]{:S(2)}, u32[]{:S(2)}) collective-permute-start(bf16[24,2048]{1,0:T(8,128)(2,1)} %get-tuple-element.16), channel_id=1, source_target_pairs={{0,10},{2,12},{4,14},{6,0},{8,2},{10,4},{12,6},{14,8},{1,11},{3,13... | collective-permute-start | bytes 294920 | tf_op jit(solution)/shard_map/ppermute | solution.py:25
  117.1 2.2 collective-permute-start.11
  119.4 1.0 fusion.22
  120.4 5.1 %collective-permute-start.12 = (bf16[24,2048]{1,0:T(8,128)(2,1)}, bf16[24,2048]{1,0:T(8,128)(2,1)}, u32[]{:S(2)}, u32[]{:S(2)}) collective-permute-start(bf16[24,2048]{1,0:T(8,128)(2,1)} %get-tuple-element.14), channel_id=1, source_target_pairs={{0,12},{2,14},{4,0},{6,2},{8,4},{10,6},{12,8},{14,10},{1,13},{3,15... | collective-permute-start | bytes 294920 | tf_op jit(solution)/shard_map/ppermute | solution.py:25
  125.6 2.2 collective-permute-start.13
  127.8 4.3 %collective-permute-start.14 = (bf16[24,2048]{1,0:T(8,128)(2,1)S(1)}, bf16[24,2048]{1,0:T(8,128)(2,1)}, u32[]{:S(2)}, u32[]{:S(2)}) collective-permute-start(bf16[24,2048]{1,0:T(8,128)(2,1)S(1)} %get-tuple-element.12), channel_id=1, source_target_pairs={{0,14},{2,0},{4,2},{6,4},{8,6},{10,8},{12,10},{14,12},{1,15},{3,1}... | collective-permute-start | bytes 294920 | tf_op jit(solution)/shard_map/ppermute | solution.py:25
  132.1 3.0 %collective-permute-start.8 = (bf16[24,2048]{1,0:T(8,128)(2,1)S(1)}, bf16[24,2048]{1,0:T(8,128)(2,1)}, u32[]{:S(2)}, u32[]{:S(2)}) collective-permute-start(bf16[24,2048]{1,0:T(8,128)(2,1)S(1)} %get-tuple-element.11), channel_id=1, source_target_pairs={{0,8},{2,10},{4,12},{6,14},{8,0},{10,2},{12,4},{14,6},{1,9},{3,11}... | collective-permute-start | bytes 294920 | tf_op jit(solution)/shard_map/ppermute | solution.py:25
  135.1 3.8 %collective-permute-start.9 = (bf16[24,2048]{1,0:T(8,128)(2,1)S(1)}, bf16[24,2048]{1,0:T(8,128)(2,1)}, u32[]{:S(2)}, u32[]{:S(2)}) collective-permute-start(bf16[24,2048]{1,0:T(8,128)(2,1)S(1)} %get-tuple-element.17), channel_id=1, source_target_pairs={{0,6},{2,8},{4,10},{6,12},{8,14},{10,0},{12,2},{14,4},{1,7},{3,9},... | collective-permute-start | bytes 294920 | tf_op jit(solution)/shard_map/ppermute | solution.py:25
  139.0 2.8 %collective-permute-done.8 = bf16[24,2048]{1,0:T(8,128)(2,1)} collective-permute-done((bf16[24,2048]{1,0:T(8,128)(2,1)S(1)}, bf16[24,2048]{1,0:T(8,128)(2,1)}, u32[]{:S(2)}, u32[]{:S(2)}) %collective-permute-start.8) | collective-permute-done | bytes 98336 | tf_op jit(solution)/shard_map/ppermute | solution.py:25
  141.8 6.8 %collective-permute-done.9 = bf16[24,2048]{1,0:T(8,128)(2,1)} collective-permute-done((bf16[24,2048]{1,0:T(8,128)(2,1)S(1)}, bf16[24,2048]{1,0:T(8,128)(2,1)}, u32[]{:S(2)}, u32[]{:S(2)}) %collective-permute-start.9) | collective-permute-done | bytes 98336 | tf_op jit(solution)/shard_map/ppermute | solution.py:25
  148.6 1.5 fusion.18
  150.2 1.6 bitcast_dynamic-update-slice_fusion.15
  151.9 1.9 collective-permute-start.15
  153.8 3.4 %collective-permute-start.16 = (bf16[1,24,2048]{2,1,0:T(8,128)(2,1)}, bf16[1,24,2048]{2,1,0:T(8,128)(2,1)S(1)}, u32[]{:S(2)}, u32[]{:S(2)}) collective-permute-start(bf16[1,24,2048]{2,1,0:T(8,128)(2,1)} %bitcast.32), channel_id=1, source_target_pairs={{0,2},{2,4},{4,6},{6,8},{8,10},{10,12},{12,14},{14,0},{1,3},{3,5},... | collective-permute-start | bytes 294920 | tf_op jit(solution)/shard_map/ppermute | solution.py:25
  157.2 10.6 %all-to-all-start.3 = ((bf16[64,32,256]{2,1,0:T(8,128)(2,1)}), bf16[64,32,256]{2,1,0:T(8,128)(2,1)S(1)}, u32[]{:S(2)}, u32[]{:S(2)}) async-start(bf16[64,32,256]{2,1,0:T(8,128)(2,1)} %bitcast.92), calls=%async_computation.3 | async-start | bytes 2097152 | tf_op jit(solution)/shard_map/all_to_all | solution.py:16
  167.8 3.1 %collective-permute-start.17 = (bf16[1,24,2048]{2,1,0:T(8,128)(2,1)}, bf16[1,24,2048]{2,1,0:T(8,128)(2,1)S(1)}, u32[]{:S(2)}, u32[]{:S(2)}) collective-permute-start(bf16[1,24,2048]{2,1,0:T(8,128)(2,1)} %collective-permute-done.15), channel_id=1, source_target_pairs={{0,14},{2,0},{4,2},{6,4},{8,6},{10,8},{12,10},{14,12},{1,15},{3,1}... | collective-permute-start | bytes 294920 | tf_op jit(solution)/shard_map/ppermute | solution.py:25
  171.0 2.2 collective-permute-start.18
  173.1 0.9 bitcast_dynamic-update-slice_fusion.14
  174.1 4.3 %collective-permute-start.19 = (bf16[1,24,2048]{2,1,0:T(8,128)(2,1)S(1)}, bf16[1,24,2048]{2,1,0:T(8,128)(2,1)S(1)}, u32[]{:S(2)}, u32[]{:S(2)}) collective-permute-start(bf16[1,24,2048]{2,1,0:T(8,128)(2,1)S(1)} %collective-permute-done.17), channel_id=1, source_target_pairs={{0,14},{2,0},{4,2},{6,4},{8,6},{10,8},{12,10},{14,12},{1,15},{3,1}... | collective-permute-start | bytes 294920 | tf_op jit(solution)/shard_map/ppermute | solution.py:25
  178.4 1.9 collective-permute-start.20
  180.4 4.9 %collective-permute-done.20 = bf16[1,24,2048]{2,1,0:T(8,128)(2,1)S(1)} collective-permute-done((bf16[1,24,2048]{2,1,0:T(8,128)(2,1)S(1)}, bf16[1,24,2048]{2,1,0:T(8,128)(2,1)S(1)}, u32[]{:S(2)}, u32[]{:S(2)}) %collective-permute-start.20) | collective-permute-done | bytes 98336 | tf_op jit(solution)/shard_map/ppermute | solution.py:25
  185.3 1.9 collective-permute-start.21
  187.3 4.9 %collective-permute-done.21 = bf16[1,24,2048]{2,1,0:T(8,128)(2,1)S(1)} collective-permute-done((bf16[1,24,2048]{2,1,0:T(8,128)(2,1)S(1)}, bf16[1,24,2048]{2,1,0:T(8,128)(2,1)S(1)}, u32[]{:S(2)}, u32[]{:S(2)}) %collective-permute-start.21) | collective-permute-done | bytes 98336 | tf_op jit(solution)/shard_map/ppermute | solution.py:25
  192.2 7.9 %collective-permute-start.22 = (bf16[1,192,2048]{2,1,0:T(8,128)(2,1)S(1)}, bf16[1,192,2048]{2,1,0:T(8,128)(2,1)}, u32[]{:S(2)}, u32[]{:S(2)}) collective-permute-start(bf16[1,192,2048]{2,1,0:T(8,128)(2,1)S(1)} %bitcast.93), channel_id=1, source_target_pairs={{0,1},{1,0},{2,3},{3,2},{4,5},{5,4},{6,7},{7,6},{8,9},{9,8},{10,11... | collective-permute-start | bytes 2359304 | tf_op jit(solution)/shard_map/ppermute | solution.py:29
  200.3 23.3 %all_to_all.26 = f32[64,1,256]{2,1,0:T(1,128)S(1)} all-to-all(f32[64,1,256]{2,1,0:T(1,128)S(1)} %broadcast_in_dim.96), channel_id=1, replica_groups=mesh['z'=8,'y'=8,'x'=8,'c'=2] {'z','y'}, dimensions={0} | all-to-all | bytes 131072 | tf_op jit(solution)/shard_map/all_to_all | solution.py:16
  224.5 1.2 constant_dynamic-update-slice_fusion
  225.8 1.1 copy-done.2
  (51 shorter events, 3.5 us)
Async XLA Ops:
  0.6 88.4 %copy-start = (bf16[384,2048]{1,0:T(8,128)(2,1)S(1)}, bf16[384,2048]{1,0:T(8,128)(2,1)}, u32[]{:S(2)}) copy-start(bf16[384,2048]{1,0:T(8,128)(2,1)} %param.11) | copy-start | bytes 4718596
  0.6 37.3 %copy-start.6 = (bf16[256,32]{0,1:T(8,128)(2,1)S(1)}, bf16[256,32]{0,1:T(8,128)(2,1)}, u32[]{:S(2)}) copy-start(bf16[256,32]{0,1:T(8,128)(2,1)} %param.10) | copy-start | bytes 49156
  2.2 27.7 %all-to-all-start = ((bf16[8,32,512]{2,1,0:T(8,128)(2,1)}), bf16[8,32,512]{2,1,0:T(8,128)(2,1)S(1)}, u32[]{:S(2)}, u32[]{:S(2)}) async-start(bf16[8,32,512]{2,1,0:T(8,128)(2,1)} %broadcast_in_dim.76), calls=%async_computation | async-start | bytes 524288 | tf_op jit(solution)/shard_map/all_to_all | solution.py:16
  30.0 26.8 %collective-permute-start = (bf16[8,32,512]{2,1,0:T(8,128)(2,1)S(1)}, bf16[8,32,512]{2,1,0:T(8,128)(2,1)S(1)}, u32[]{:S(2)}, u32[]{:S(2)}) collective-permute-start(bf16[8,32,512]{2,1,0:T(8,128)(2,1)S(1)} %all-to-all-done), channel_id=1, source_target_pairs={{0,112},{16,0},{32,16},{48,32},{64,48},{80,64},{96,80},{112,96},{1... | collective-permute-start | bytes 786440 | tf_op jit(solution)/shard_map/ppermute | solution.py:25
  35.9 23.0 %collective-permute-start.1 = (bf16[8,32,512]{2,1,0:T(8,128)(2,1)S(1)}, bf16[8,32,512]{2,1,0:T(8,128)(2,1)S(1)}, u32[]{:S(2)}, u32[]{:S(2)}) collective-permute-start(bf16[8,32,512]{2,1,0:T(8,128)(2,1)S(1)} %all-to-all-done), channel_id=1, source_target_pairs={{0,16},{16,32},{32,48},{48,64},{64,80},{80,96},{96,112},{112,0},{1... | collective-permute-start | bytes 786440 | tf_op jit(solution)/shard_map/ppermute | solution.py:25
  38.6 12.8 %all-to-all-start.1 = ((bf16[8,32,256]{2,1,0:T(8,128)(2,1)}), bf16[8,32,256]{2,1,0:T(8,128)(2,1)S(1)}, u32[]{:S(2)}, u32[]{:S(2)}) async-start(bf16[8,32,256]{2,1,0:T(8,128)(2,1)} %broadcast_in_dim.77), calls=%async_computation.1 | async-start | bytes 262144 | tf_op jit(solution)/shard_map/all_to_all | solution.py:16
  52.5 38.7 %all-to-all-start.2 = ((bf16[8,8,32,256]{3,2,1,0:T(8,128)(2,1)}), bf16[8,8,32,256]{3,2,1,0:T(8,128)(2,1)}, u32[]{:S(2)}, u32[]{:S(2)}) async-start(bf16[8,8,32,256]{3,2,1,0:T(8,128)(2,1)} %broadcast_in_dim.78), calls=%async_computation.2 | async-start | bytes 2097152 | tf_op jit(solution)/shard_map/all_to_all | solution.py:16
  56.7 28.6 %copy-start.1 = (bf16[384,2048]{1,0:T(8,128)(2,1)S(1)}, bf16[384,2048]{1,0:T(8,128)(2,1)}, u32[]{:S(2)}) copy-start(bf16[384,2048]{1,0:T(8,128)(2,1)} %param.6) | copy-start | bytes 4718596
  56.7 28.6 %copy-start.7 = (f32[2048]{0:T(1024)S(1)}, f32[2048]{0:T(1024)}, u32[]{:S(2)}) copy-start(f32[2048]{0:T(1024)} %param.7) | copy-start | bytes 24580
  56.7 7.6 %collective-permute-start.2 = (bf16[8,32,512]{2,1,0:T(8,128)(2,1)S(1)}, bf16[8,32,512]{2,1,0:T(8,128)(2,1)S(1)}, u32[]{:S(2)}, u32[]{:S(2)}) collective-permute-start(bf16[8,32,512]{2,1,0:T(8,128)(2,1)S(1)} %collective-permute-done), channel_id=1, source_target_pairs={{0,112},{16,0},{32,16},{48,32},{64,48},{80,64},{96,80},{112,96},{1... | collective-permute-start | bytes 786440 | tf_op jit(solution)/shard_map/ppermute | solution.py:25
  58.8 8.3 %collective-permute-start.3 = (bf16[8,32,512]{2,1,0:T(8,128)(2,1)S(1)}, bf16[8,32,512]{2,1,0:T(8,128)(2,1)S(1)}, u32[]{:S(2)}, u32[]{:S(2)}) collective-permute-start(bf16[8,32,512]{2,1,0:T(8,128)(2,1)S(1)} %collective-permute-done.1), channel_id=1, source_target_pairs={{0,16},{16,32},{32,48},{48,64},{64,80},{80,96},{96,112},{112,0},{1... | collective-permute-start | bytes 786440 | tf_op jit(solution)/shard_map/ppermute | solution.py:25
  64.4 13.4 %collective-permute-start.4 = (bf16[8,32,512]{2,1,0:T(8,128)(2,1)S(1)}, bf16[8,32,512]{2,1,0:T(8,128)(2,1)S(1)}, u32[]{:S(2)}, u32[]{:S(2)}) collective-permute-start(bf16[8,32,512]{2,1,0:T(8,128)(2,1)S(1)} %collective-permute-done.2), channel_id=1, source_target_pairs={{0,112},{16,0},{32,16},{48,32},{64,48},{80,64},{96,80},{112,96},{1... | collective-permute-start | bytes 786440 | tf_op jit(solution)/shard_map/ppermute | solution.py:25
  67.1 8.7 %collective-permute-start.5 = (bf16[8,32,512]{2,1,0:T(8,128)(2,1)S(1)}, bf16[8,32,512]{2,1,0:T(8,128)(2,1)S(1)}, u32[]{:S(2)}, u32[]{:S(2)}) collective-permute-start(bf16[8,32,512]{2,1,0:T(8,128)(2,1)S(1)} %collective-permute-done.3), channel_id=1, source_target_pairs={{0,16},{16,32},{32,48},{48,64},{64,80},{80,96},{96,112},{112,0},{1... | collective-permute-start | bytes 786440 | tf_op jit(solution)/shard_map/ppermute | solution.py:25
  75.9 8.7 %collective-permute-start.6 = (bf16[8,32,512]{2,1,0:T(8,128)(2,1)S(1)}, bf16[8,32,512]{2,1,0:T(8,128)(2,1)S(1)}, u32[]{:S(2)}, u32[]{:S(2)}) collective-permute-start(bf16[8,32,512]{2,1,0:T(8,128)(2,1)S(1)} %collective-permute-done.5), channel_id=1, source_target_pairs={{0,16},{16,32},{32,48},{48,64},{64,80},{80,96},{96,112},{112,0},{1... | collective-permute-start | bytes 786440 | tf_op jit(solution)/shard_map/ppermute | solution.py:25
  89.0 2.1 copy-start.3
  93.0 1.9 copy-start.4
  97.7 11.0 %collective-permute-start.7 = (bf16[192,2048]{1,0:T(8,128)(2,1)}, bf16[192,2048]{1,0:T(8,128)(2,1)}, u32[]{:S(2)}, u32[]{:S(2)}) collective-permute-start(bf16[192,2048]{1,0:T(8,128)(2,1)} %dynamic-slice_bitcast_fusion), channel_id=1, source_target_pairs={{0,1},{1,0},{2,3},{3,2},{4,5},{5,4},{6,7},{7,6},{8,9},{9,8},{10,11... | collective-permute-start | bytes 2359304 | tf_op jit(solution)/shard_map/ppermute | solution.py:29
  110.9 21.2 %collective-permute-start.10 = (bf16[24,2048]{1,0:T(8,128)(2,1)}, bf16[24,2048]{1,0:T(8,128)(2,1)}, u32[]{:S(2)}, u32[]{:S(2)}) collective-permute-start(bf16[24,2048]{1,0:T(8,128)(2,1)} %get-tuple-element.16), channel_id=1, source_target_pairs={{0,10},{2,12},{4,14},{6,0},{8,2},{10,4},{12,6},{14,8},{1,11},{3,13... | collective-permute-start | bytes 294920 | tf_op jit(solution)/shard_map/ppermute | solution.py:25
  117.1 18.0 %collective-permute-start.11 = (bf16[24,2048]{1,0:T(8,128)(2,1)}, bf16[24,2048]{1,0:T(8,128)(2,1)}, u32[]{:S(2)}, u32[]{:S(2)}) collective-permute-start(bf16[24,2048]{1,0:T(8,128)(2,1)} %get-tuple-element.15), channel_id=1, source_target_pairs={{0,4},{2,6},{4,8},{6,10},{8,12},{10,14},{12,0},{14,2},{1,5},{3,7},... | collective-permute-start | bytes 294920 | tf_op jit(solution)/shard_map/ppermute | solution.py:25
  120.4 18.5 %collective-permute-start.12 = (bf16[24,2048]{1,0:T(8,128)(2,1)}, bf16[24,2048]{1,0:T(8,128)(2,1)}, u32[]{:S(2)}, u32[]{:S(2)}) collective-permute-start(bf16[24,2048]{1,0:T(8,128)(2,1)} %get-tuple-element.14), channel_id=1, source_target_pairs={{0,12},{2,14},{4,0},{6,2},{8,4},{10,6},{12,8},{14,10},{1,13},{3,15... | collective-permute-start | bytes 294920 | tf_op jit(solution)/shard_map/ppermute | solution.py:25
  125.6 13.4 %collective-permute-start.13 = (bf16[24,2048]{1,0:T(8,128)(2,1)S(1)}, bf16[24,2048]{1,0:T(8,128)(2,1)}, u32[]{:S(2)}, u32[]{:S(2)}) collective-permute-start(bf16[24,2048]{1,0:T(8,128)(2,1)S(1)} %get-tuple-element.13), channel_id=1, source_target_pairs={{0,2},{2,4},{4,6},{6,8},{8,10},{10,12},{12,14},{14,0},{1,3},{3,5},... | collective-permute-start | bytes 294920 | tf_op jit(solution)/shard_map/ppermute | solution.py:25
  127.8 11.2 %collective-permute-start.14 = (bf16[24,2048]{1,0:T(8,128)(2,1)S(1)}, bf16[24,2048]{1,0:T(8,128)(2,1)}, u32[]{:S(2)}, u32[]{:S(2)}) collective-permute-start(bf16[24,2048]{1,0:T(8,128)(2,1)S(1)} %get-tuple-element.12), channel_id=1, source_target_pairs={{0,14},{2,0},{4,2},{6,4},{8,6},{10,8},{12,10},{14,12},{1,15},{3,1}... | collective-permute-start | bytes 294920 | tf_op jit(solution)/shard_map/ppermute | solution.py:25
  132.1 9.7 %collective-permute-start.8 = (bf16[24,2048]{1,0:T(8,128)(2,1)S(1)}, bf16[24,2048]{1,0:T(8,128)(2,1)}, u32[]{:S(2)}, u32[]{:S(2)}) collective-permute-start(bf16[24,2048]{1,0:T(8,128)(2,1)S(1)} %get-tuple-element.11), channel_id=1, source_target_pairs={{0,8},{2,10},{4,12},{6,14},{8,0},{10,2},{12,4},{14,6},{1,9},{3,11}... | collective-permute-start | bytes 294920 | tf_op jit(solution)/shard_map/ppermute | solution.py:25
  135.1 13.5 %collective-permute-start.9 = (bf16[24,2048]{1,0:T(8,128)(2,1)S(1)}, bf16[24,2048]{1,0:T(8,128)(2,1)}, u32[]{:S(2)}, u32[]{:S(2)}) collective-permute-start(bf16[24,2048]{1,0:T(8,128)(2,1)S(1)} %get-tuple-element.17), channel_id=1, source_target_pairs={{0,6},{2,8},{4,10},{6,12},{8,14},{10,0},{12,2},{14,4},{1,7},{3,9},... | collective-permute-start | bytes 294920 | tf_op jit(solution)/shard_map/ppermute | solution.py:25
  151.9 16.0 %collective-permute-start.15 = (bf16[1,24,2048]{2,1,0:T(8,128)(2,1)}, bf16[1,24,2048]{2,1,0:T(8,128)(2,1)}, u32[]{:S(2)}, u32[]{:S(2)}) collective-permute-start(bf16[1,24,2048]{2,1,0:T(8,128)(2,1)} %bitcast.32), channel_id=1, source_target_pairs={{0,14},{2,0},{4,2},{6,4},{8,6},{10,8},{12,10},{14,12},{1,15},{3,1}... | collective-permute-start | bytes 294920 | tf_op jit(solution)/shard_map/ppermute | solution.py:25
  153.8 17.2 %collective-permute-start.16 = (bf16[1,24,2048]{2,1,0:T(8,128)(2,1)}, bf16[1,24,2048]{2,1,0:T(8,128)(2,1)S(1)}, u32[]{:S(2)}, u32[]{:S(2)}) collective-permute-start(bf16[1,24,2048]{2,1,0:T(8,128)(2,1)} %bitcast.32), channel_id=1, source_target_pairs={{0,2},{2,4},{4,6},{6,8},{8,10},{10,12},{12,14},{14,0},{1,3},{3,5},... | collective-permute-start | bytes 294920 | tf_op jit(solution)/shard_map/ppermute | solution.py:25
  157.2 42.8 %all-to-all-start.3 = ((bf16[64,32,256]{2,1,0:T(8,128)(2,1)}), bf16[64,32,256]{2,1,0:T(8,128)(2,1)S(1)}, u32[]{:S(2)}, u32[]{:S(2)}) async-start(bf16[64,32,256]{2,1,0:T(8,128)(2,1)} %bitcast.92), calls=%async_computation.3 | async-start | bytes 2097152 | tf_op jit(solution)/shard_map/all_to_all | solution.py:16
  167.8 6.2 %collective-permute-start.17 = (bf16[1,24,2048]{2,1,0:T(8,128)(2,1)}, bf16[1,24,2048]{2,1,0:T(8,128)(2,1)S(1)}, u32[]{:S(2)}, u32[]{:S(2)}) collective-permute-start(bf16[1,24,2048]{2,1,0:T(8,128)(2,1)} %collective-permute-done.15), channel_id=1, source_target_pairs={{0,14},{2,0},{4,2},{6,4},{8,6},{10,8},{12,10},{14,12},{1,15},{3,1}... | collective-permute-start | bytes 294920 | tf_op jit(solution)/shard_map/ppermute | solution.py:25
  171.0 7.4 %collective-permute-start.18 = (bf16[1,24,2048]{2,1,0:T(8,128)(2,1)S(1)}, bf16[1,24,2048]{2,1,0:T(8,128)(2,1)S(1)}, u32[]{:S(2)}, u32[]{:S(2)}) collective-permute-start(bf16[1,24,2048]{2,1,0:T(8,128)(2,1)S(1)} %collective-permute-done.16), channel_id=1, source_target_pairs={{0,2},{2,4},{4,6},{6,8},{8,10},{10,12},{12,14},{14,0},{1,3},{3,5},... | collective-permute-start | bytes 294920 | tf_op jit(solution)/shard_map/ppermute | solution.py:25
  174.1 13.1 %collective-permute-start.19 = (bf16[1,24,2048]{2,1,0:T(8,128)(2,1)S(1)}, bf16[1,24,2048]{2,1,0:T(8,128)(2,1)S(1)}, u32[]{:S(2)}, u32[]{:S(2)}) collective-permute-start(bf16[1,24,2048]{2,1,0:T(8,128)(2,1)S(1)} %collective-permute-done.17), channel_id=1, source_target_pairs={{0,14},{2,0},{4,2},{6,4},{8,6},{10,8},{12,10},{14,12},{1,15},{3,1}... | collective-permute-start | bytes 294920 | tf_op jit(solution)/shard_map/ppermute | solution.py:25
  178.4 6.9 %collective-permute-start.20 = (bf16[1,24,2048]{2,1,0:T(8,128)(2,1)S(1)}, bf16[1,24,2048]{2,1,0:T(8,128)(2,1)S(1)}, u32[]{:S(2)}, u32[]{:S(2)}) collective-permute-start(bf16[1,24,2048]{2,1,0:T(8,128)(2,1)S(1)} %collective-permute-done.18), channel_id=1, source_target_pairs={{0,2},{2,4},{4,6},{6,8},{8,10},{10,12},{12,14},{14,0},{1,3},{3,5},... | collective-permute-start | bytes 294920 | tf_op jit(solution)/shard_map/ppermute | solution.py:25
  185.3 6.9 %collective-permute-start.21 = (bf16[1,24,2048]{2,1,0:T(8,128)(2,1)S(1)}, bf16[1,24,2048]{2,1,0:T(8,128)(2,1)S(1)}, u32[]{:S(2)}, u32[]{:S(2)}) collective-permute-start(bf16[1,24,2048]{2,1,0:T(8,128)(2,1)S(1)} %collective-permute-done.20), channel_id=1, source_target_pairs={{0,2},{2,4},{4,6},{6,8},{8,10},{10,12},{12,14},{14,0},{1,3},{3,5},... | collective-permute-start | bytes 294920 | tf_op jit(solution)/shard_map/ppermute | solution.py:25
  192.2 32.4 %collective-permute-start.22 = (bf16[1,192,2048]{2,1,0:T(8,128)(2,1)S(1)}, bf16[1,192,2048]{2,1,0:T(8,128)(2,1)}, u32[]{:S(2)}, u32[]{:S(2)}) collective-permute-start(bf16[1,192,2048]{2,1,0:T(8,128)(2,1)S(1)} %bitcast.93), channel_id=1, source_target_pairs={{0,1},{1,0},{2,3},{3,2},{4,5},{5,4},{6,7},{7,6},{8,9},{9,8},{10,11... | collective-permute-start | bytes 2359304 | tf_op jit(solution)/shard_map/ppermute | solution.py:29
  200.2 25.5 %copy-start.5 = (f32[32,256]{1,0:T(8,128)}, f32[32,256]{1,0:T(8,128)S(1)}, u32[]{:S(2)}) copy-start(f32[32,256]{1,0:T(8,128)S(1)} %convert_reduce_fusion) | copy-start | bytes 98308
  225.8 1.1 copy-start.2
where the time goes:
time: 228 us; the launch traced here: 227 us
  starting transfers between devices  119 us (52%)
  waiting for transfers between devices  46.6 us (20%)
  blocking collectives  23.3 us (10%)
  local copies, waits for them, and re-layouts  16.1 us (7%)
  matrix products  10.1 us (4%)
  other arithmetic  9.85 us (4%)
    ppermute x21, starting transfers between devices, shift(): lax.ppermute(value, axis, [(i, (i + by) % peers) for i in range(peers)])  66 us
    all_to_all x4, starting transfers between devices, swap(): return lax.all_to_all(pieces, axis, split_axis=0, concat_axis=0, tiled=True)  36.8 us
    ppermute x21, waiting for transfers between devices, shift(): lax.ppermute(value, axis, [(i, (i + by) % peers) for i in range(peers)])  30.1 us
    all_to_all x1, blocking collectives, swap(): return lax.all_to_all(pieces, axis, split_axis=0, concat_axis=0, tiled=True)  23.3 us
    ppermute x2, starting transfers between devices, exchange(): lax.ppermute(value, axis, [(i, i ^ bit) for i in range(lax.axis_size(axis...  16.6 us
    all_to_all x4, waiting for transfers between devices, swap(): return lax.all_to_all(pieces, axis, split_axis=0, concat_axis=0, tiled=True)  14.4 us
    dynamic_update_slice x15, local copies, waits for them, and re-layouts, put(): lax.dynamic_update_slice(whole, piece[:, None], (0, index % peers, 0, 0))  7.02 us
  transfers between devices with their start and end apart: 27, of which 10 were waited for; matrix products, arithmetic and copies ran while one was open for 9% of the time, Pallas kernels for 0%

commit v1 on v0

--- a/solution.py
+++ b/solution.py
@@ -58,17 +58,16 @@
     part_rows, units = w_gate.shape
     sizes = {a: lax.axis_size(a) for a in ("z", "y", "x", "c")}
 
+    down = copy_for_each(w_down.T, "y")
     both = copy_for_each(jnp.concatenate([w_gate, w_up], axis=1), "z")
-    down = copy_for_each(after(w_down.T, both), "y")
     full_down = copy_for_each(down, "z").reshape(width, units)
     both = ring(both, "y").reshape(width, 2 * units)
-    full_gate, full_up = both[:, :units], both[:, units:]
 
     xf = tokens.astype(f32)
     inv = lax.rsqrt(jnp.mean(xf * xf, axis=-1, keepdims=True) + EPS)
-    normed = (xf * inv * norm_gain).astype(bf16)
-    gate = jnp.dot(normed, full_gate, preferred_element_type=f32)
-    up = jnp.dot(normed, full_up, preferred_element_type=f32)
+    normed = lax.optimization_barrier((xf * inv * norm_gain).astype(bf16))
+    hidden_in = jnp.dot(normed, both, preferred_element_type=f32)
+    gate, up = hidden_in[:, :units], hidden_in[:, units:]
     sig = jax.nn.sigmoid(gate)
     act = gate * sig
     hidden = (act * up).astype(bf16)
@@ -76,18 +75,16 @@
     down_part = 0.5 * lax.dot_general(
         cotangent, hidden, (((0,), (0,)), ((), ())), preferred_element_type=f32
     )
-    down_part = down_part.astype(bf16).reshape(-1, part_rows, units)
-    down_pieces = swap(down_part, FS)
+    down_part = down_part.astype(bf16).reshape(sizes["z"], -1, units)
+    down_pieces = swap(down_part, "z")
 
     full_down = after(full_down, down_part)
     d_hidden = 0.5 * jnp.dot(cotangent, full_down, preferred_element_type=f32)
     d_gate = (d_hidden * up * sig * (1.0 + gate * (1.0 - sig))).astype(bf16)
     d_up = (d_hidden * act).astype(bf16)
 
-    part = lax.dot_general(d_gate, full_gate, (((1,), (1,)), ((), ())), preferred_element_type=f32)
-    part = part + lax.dot_general(
-        d_up, full_up, (((1,), (1,)), ((), ())), preferred_element_type=f32
-    )
+    d_both = jnp.concatenate([d_gate, d_up], axis=1)
+    part = lax.dot_general(d_both, both, (((1,), (1,)), ((), ())), preferred_element_type=f32)
     core, place = lax.axis_index("c"), lax.axis_index("x")
     pair = part.astype(bf16).reshape(sizes["c"], rows // sizes["c"], width)
     theirs = lax.dynamic_index_in_dim(pair, 1 - core, 0, False)
@@ -103,7 +100,17 @@
 
     d_share = piece(place)
     for by in (4, 3, 5, 2, 6, 1, 7):
-        d_share = d_share + shift(piece(place + by).astype(bf16), "x", by).astype(f32)
+        got = shift(piece(place + by).astype(bf16), "x", by)
+        d_share = d_share + got.astype(f32)
+
+    along_y = jnp.sum(down_pieces.astype(f32), axis=0).astype(bf16)
+    down_pieces = swap(along_y.reshape(sizes["y"], part_rows, units), "y")
+    share = jnp.sum(down_pieces.astype(f32), axis=0)
+    norms = jnp.sum(share * share, axis=0)
+    for axis in ("y", "z"):
+        norms = copy_for_each(norms, axis)
+        norms = jnp.sum(norms, axis=0)
+
     offset = (core * sizes["x"] + place) * own
     own_tokens = lax.dynamic_slice_in_dim(tokens, offset, own, 0).astype(f32)
     own_inv = lax.rsqrt(jnp.mean(own_tokens * own_tokens, axis=-1, keepdims=True) + EPS)
@@ -111,16 +118,13 @@
     d_scaled = d_share * norm_gain
     inner = jnp.mean(d_scaled * scaled, axis=-1, keepdims=True)
     grad_own = (own_inv * (d_scaled - scaled * inner)).astype(bf16)
-    share = jnp.sum(down_pieces.astype(f32), axis=0)
-    norms = jnp.sum(share * share, axis=0)
-    norms = copy_for_each(norms, FS)
-    grad_half = ring(grad_own[None], "x").reshape(1, -1, width)
+    grad_half = copy_for_each(grad_own, "x").reshape(1, -1, width)
     others = exchange(grad_half, "c", 1)
     grad_tokens = jnp.zeros((sizes["c"], *grad_half.shape[1:]), bf16)
     grad_tokens = lax.dynamic_update_slice(grad_tokens, grad_half, (core, 0, 0))
     grad_tokens = lax.dynamic_update_slice(grad_tokens, others, (1 - core, 0, 0))
     grad_tokens = grad_tokens.reshape(rows, width)
-    return (grad_tokens, share.T, jnp.sum(norms, axis=0))
+    return (grad_tokens, share.T, norms)
 
 
 def solution(mesh):

time: 228 us -> 242 us (1.061)
  the two profiles are of different devices: /device:TPU:1 before, /device:TPU:16 now
where the time goes in v1:
time: 242 us; the launch traced here: 241 us
  starting transfers between devices  91.1 us (38%)
  waiting for transfers between devices  83.7 us (35%)
  blocking collectives  35.5 us (15%)
  local copies, waits for them, and re-layouts  13.9 us (6%)
  other arithmetic  9.27 us (4%)
  matrix products  5.87 us (2%)
    all_to_all x5, waiting for transfers between devices, swap(): return lax.all_to_all(pieces, axis, split_axis=0, concat_axis=0, tiled=True)  55.7 us
    ppermute x14, starting transfers between devices, shift(): lax.ppermute(value, axis, [(i, (i + by) % peers) for i in range(peers)])  47.8 us
    all_to_all x5, starting transfers between devices, swap(): return lax.all_to_all(pieces, axis, split_axis=0, concat_axis=0, tiled=True)  39.5 us
    all_to_all x3, blocking collectives, swap(): return lax.all_to_all(pieces, axis, split_axis=0, concat_axis=0, tiled=True)  35.5 us
    ppermute x14, waiting for transfers between devices, shift(): lax.ppermute(value, axis, [(i, (i + by) % peers) for i in range(peers)])  25.6 us
  transfers between devices with their start and end apart: 21, of which 11 were waited for; matrix products, arithmetic and copies ran while one was open for 5% of the time, Pallas kernels for 0%

profile of v1, /device:TPU:16, one launch (start us, length us, event | category | flops | bytes accessed | tf_op | source)
XLA Modules:
  0.0 240.6 jit_solution(16697988394950640211)
XLA Ops:
  0.7 0.9 pad_maximum_fusion
  1.6 0.7 broadcast_in_dim.57
  2.3 16.7 %all-to-all-start.2 = ((bf16[8,32,512]{2,1,0:T(8,128)(2,1)}), bf16[8,32,512]{2,1,0:T(8,128)(2,1)S(1)}, u32[]{:S(2)}, u32[]{:S(2)}) async-start(bf16[8,32,512]{2,1,0:T(8,128)(2,1)} %broadcast_in_dim.57), calls=%async_computation.2 | async-start | bytes 524288 | tf_op jit(solution)/shard_map/all_to_all | solution.py:16
  19.0 1.8 fusion
  20.8 10.1 %all-to-all-done.2 = bf16[8,32,512]{2,1,0:T(8,128)(2,1)S(1)} async-done(((bf16[8,32,512]{2,1,0:T(8,128)(2,1)}), bf16[8,32,512]{2,1,0:T(8,128)(2,1)S(1)}, u32[]{:S(2)}, u32[]{:S(2)}) %all-to-all-start.2) | async-done | bytes 262176 | tf_op jit(solution)/shard_map/all_to_all | solution.py:16
  30.9 0.7 broadcast_in_dim.54
  31.5 7.9 %all-to-all-start = ((bf16[8,32,256]{2,1,0:T(8,128)(2,1)}), bf16[8,32,256]{2,1,0:T(8,128)(2,1)S(1)}, u32[]{:S(2)}, u32[]{:S(2)}) async-start(bf16[8,32,256]{2,1,0:T(8,128)(2,1)} %broadcast_in_dim.54), calls=%async_computation | async-start | bytes 262144 | tf_op jit(solution)/shard_map/all_to_all | solution.py:16
  39.4 1.9 collective-permute-start
  41.3 3.9 %collective-permute-start.1 = (bf16[8,32,512]{2,1,0:T(8,128)(2,1)S(1)}, bf16[8,32,512]{2,1,0:T(8,128)(2,1)}, u32[]{:S(2)}, u32[]{:S(2)}) collective-permute-start(bf16[8,32,512]{2,1,0:T(8,128)(2,1)S(1)} %all-to-all-done.2), channel_id=1, source_target_pairs={{0,16},{16,32},{32,48},{48,64},{64,80},{80,96},{96,112},{112,0},{1... | collective-permute-start | bytes 786440 | tf_op jit(solution)/shard_map/ppermute | solution.py:25
  45.3 1.6 fusion.2
  46.8 0.9 all-to-all-done
  47.7 1.1 broadcast_in_dim.55
  48.9 4.2 %all-to-all-start.1 = ((bf16[8,8,32,256]{3,2,1,0:T(8,128)(2,1)}), bf16[8,8,32,256]{3,2,1,0:T(8,128)(2,1)}, u32[]{:S(2)}, u32[]{:S(2)}) async-start(bf16[8,8,32,256]{3,2,1,0:T(8,128)(2,1)} %broadcast_in_dim.55), calls=%async_computation.1 | async-start | bytes 2097152 | tf_op jit(solution)/shard_map/all_to_all | solution.py:16
  53.1 0.2 broadcast_in_dim.56
  53.4 2.9 %collective-permute-start.2 = (bf16[8,32,512]{2,1,0:T(8,128)(2,1)}, bf16[8,32,512]{2,1,0:T(8,128)(2,1)S(1)}, u32[]{:S(2)}, u32[]{:S(2)}) collective-permute-start(bf16[8,32,512]{2,1,0:T(8,128)(2,1)} %collective-permute-done), channel_id=1, source_target_pairs={{0,112},{16,0},{32,16},{48,32},{64,48},{80,64},{96,80},{112,96},{1... | collective-permute-start | bytes 786440 | tf_op jit(solution)/shard_map/ppermute | solution.py:25
  56.3 3.1 %collective-permute-start.3 = (bf16[8,32,512]{2,1,0:T(8,128)(2,1)}, bf16[8,32,512]{2,1,0:T(8,128)(2,1)S(1)}, u32[]{:S(2)}, u32[]{:S(2)}) collective-permute-start(bf16[8,32,512]{2,1,0:T(8,128)(2,1)} %collective-permute-done.1), channel_id=1, source_target_pairs={{0,16},{16,32},{32,48},{48,64},{64,80},{80,96},{96,112},{112,0},{1... | collective-permute-start | bytes 786440 | tf_op jit(solution)/shard_map/ppermute | solution.py:25
  59.4 1.0 bitcast_dynamic-update-slice_fusion.5
  60.4 1.0 bitcast_dynamic-update-slice_fusion.4
  61.4 0.7 collective-permute-done.2
  62.0 3.1 %collective-permute-start.4 = (bf16[8,32,512]{2,1,0:T(8,128)(2,1)S(1)}, bf16[8,32,512]{2,1,0:T(8,128)(2,1)S(1)}, u32[]{:S(2)}, u32[]{:S(2)}) collective-permute-start(bf16[8,32,512]{2,1,0:T(8,128)(2,1)S(1)} %collective-permute-done.2), channel_id=1, source_target_pairs={{0,112},{16,0},{32,16},{48,32},{64,48},{80,64},{96,80},{112,96},{1... | collective-permute-start | bytes 786440 | tf_op jit(solution)/shard_map/ppermute | solution.py:25
  65.1 0.4 collective-permute-done.3
  65.5 2.4 collective-permute-start.5
  67.9 7.0 %collective-permute-done.5 = bf16[8,32,512]{2,1,0:T(8,128)(2,1)S(1)} collective-permute-done((bf16[8,32,512]{2,1,0:T(8,128)(2,1)S(1)}, bf16[8,32,512]{2,1,0:T(8,128)(2,1)S(1)}, u32[]{:S(2)}, u32[]{:S(2)}) %collective-permute-start.5) | collective-permute-done | bytes 262176 | tf_op jit(solution)/shard_map/ppermute | solution.py:25
  75.0 1.9 collective-permute-start.6
  77.0 7.5 %collective-permute-done.6 = bf16[8,32,512]{2,1,0:T(8,128)(2,1)S(1)} collective-permute-done((bf16[8,32,512]{2,1,0:T(8,128)(2,1)S(1)}, bf16[8,32,512]{2,1,0:T(8,128)(2,1)S(1)}, u32[]{:S(2)}, u32[]{:S(2)}) %collective-permute-start.6) | collective-permute-done | bytes 262176 | tf_op jit(solution)/shard_map/ppermute | solution.py:25
  84.5 1.3 copy-done.4
  85.8 1.9 fusion.35
  87.7 2.2 multiply_convert_fusion.1
  89.9 1.0 convolution_convert_fusion
  90.9 1.1 copy-done.6
  92.1 1.0 dynamic-slice_bitcast_fusion
  93.0 1.9 collective-permute-start.7
  95.1 2.5 %collective-permute-done.7 = bf16[192,2048]{1,0:T(8,128)(2,1)} collective-permute-done((bf16[192,2048]{1,0:T(8,128)(2,1)}, bf16[192,2048]{1,0:T(8,128)(2,1)}, u32[]{:S(2)}, u32[]{:S(2)}) %collective-permute-start.7) | collective-permute-done | bytes 786464 | tf_op jit(solution)/shard_map/ppermute | solution.py:29
  97.6 2.4 %fusion.22 = (bf16[24,2048]{1,0:T(8,128)(2,1)S(1)}, bf16[24,2048]{1,0:T(8,128)(2,1)S(1)}, bf16[24,2048]{1,0:T(8,128)(2,1)S(1)}, bf16[24,2048]{1,0:T(8,128)(2,1)}...) fusion(bf16[192,2048]{1,0:T(8,128)(2,1)} %collective-permute-done.7, ...), kind=kLoop, calls=%fused_computation.51 | loop fusion | flops 1376256 | bytes 2064444 | tf_op jit(solution)/shard_map/convert_element_type | solution.py:103
  100.0 6.5 %collective-permute-start.10 = (bf16[24,2048]{1,0:T(8,128)(2,1)}, bf16[24,2048]{1,0:T(8,128)(2,1)}, u32[]{:S(2)}, u32[]{:S(2)}) collective-permute-start(bf16[24,2048]{1,0:T(8,128)(2,1)} %get-tuple-element.12), channel_id=1, source_target_pairs={{0,10},{2,12},{4,14},{6,0},{8,2},{10,4},{12,6},{14,8},{1,11},{3,13... | collective-permute-start | bytes 294920 | tf_op jit(solution)/shard_map/ppermute | solution.py:25
  106.5 2.5 %collective-permute-start.11 = (bf16[24,2048]{1,0:T(8,128)(2,1)}, bf16[24,2048]{1,0:T(8,128)(2,1)}, u32[]{:S(2)}, u32[]{:S(2)}) collective-permute-start(bf16[24,2048]{1,0:T(8,128)(2,1)} %get-tuple-element.11), channel_id=1, source_target_pairs={{0,4},{2,6},{4,8},{6,10},{8,12},{10,14},{12,0},{14,2},{1,5},{3,7},... | collective-permute-start | bytes 294920 | tf_op jit(solution)/shard_map/ppermute | solution.py:25
  109.0 0.1 fusion.15
  109.2 5.4 %collective-permute-start.12 = (bf16[24,2048]{1,0:T(8,128)(2,1)}, bf16[24,2048]{1,0:T(8,128)(2,1)}, u32[]{:S(2)}, u32[]{:S(2)}) collective-permute-start(bf16[24,2048]{1,0:T(8,128)(2,1)} %get-tuple-element.10), channel_id=1, source_target_pairs={{0,12},{2,14},{4,0},{6,2},{8,4},{10,6},{12,8},{14,10},{1,13},{3,15... | collective-permute-start | bytes 294920 | tf_op jit(solution)/shard_map/ppermute | solution.py:25
  114.6 2.5 %collective-permute-start.13 = (bf16[24,2048]{1,0:T(8,128)(2,1)S(1)}, bf16[24,2048]{1,0:T(8,128)(2,1)}, u32[]{:S(2)}, u32[]{:S(2)}) collective-permute-start(bf16[24,2048]{1,0:T(8,128)(2,1)S(1)} %get-tuple-element.9), channel_id=1, source_target_pairs={{0,2},{2,4},{4,6},{6,8},{8,10},{10,12},{12,14},{14,0},{1,3},{3,5},... | collective-permute-start | bytes 294920 | tf_op jit(solution)/shard_map/ppermute | solution.py:25
  117.1 4.5 %collective-permute-start.14 = (bf16[24,2048]{1,0:T(8,128)(2,1)S(1)}, bf16[24,2048]{1,0:T(8,128)(2,1)}, u32[]{:S(2)}, u32[]{:S(2)}) collective-permute-start(bf16[24,2048]{1,0:T(8,128)(2,1)S(1)} %get-tuple-element.8), channel_id=1, source_target_pairs={{0,14},{2,0},{4,2},{6,4},{8,6},{10,8},{12,10},{14,12},{1,15},{3,1}... | collective-permute-start | bytes 294920 | tf_op jit(solution)/shard_map/ppermute | solution.py:25
  121.7 3.3 %collective-permute-start.8 = (bf16[24,2048]{1,0:T(8,128)(2,1)S(1)}, bf16[24,2048]{1,0:T(8,128)(2,1)}, u32[]{:S(2)}, u32[]{:S(2)}) collective-permute-start(bf16[24,2048]{1,0:T(8,128)(2,1)S(1)} %get-tuple-element.7), channel_id=1, source_target_pairs={{0,8},{2,10},{4,12},{6,14},{8,0},{10,2},{12,4},{14,6},{1,9},{3,11}... | collective-permute-start | bytes 294920 | tf_op jit(solution)/shard_map/ppermute | solution.py:25
  125.0 3.8 %collective-permute-start.9 = (bf16[24,2048]{1,0:T(8,128)(2,1)S(1)}, bf16[24,2048]{1,0:T(8,128)(2,1)}, u32[]{:S(2)}, u32[]{:S(2)}) collective-permute-start(bf16[24,2048]{1,0:T(8,128)(2,1)S(1)} %get-tuple-element.13), channel_id=1, source_target_pairs={{0,6},{2,8},{4,10},{6,12},{8,14},{10,0},{12,2},{14,4},{1,7},{3,9},... | collective-permute-start | bytes 294920 | tf_op jit(solution)/shard_map/ppermute | solution.py:25
  128.9 7.0 %collective-permute-done.8 = bf16[24,2048]{1,0:T(8,128)(2,1)} collective-permute-done((bf16[24,2048]{1,0:T(8,128)(2,1)S(1)}, bf16[24,2048]{1,0:T(8,128)(2,1)}, u32[]{:S(2)}, u32[]{:S(2)}) %collective-permute-start.8) | collective-permute-done | bytes 98336 | tf_op jit(solution)/shard_map/ppermute | solution.py:25
  135.9 3.0 %collective-permute-done.9 = bf16[24,2048]{1,0:T(8,128)(2,1)} collective-permute-done((bf16[24,2048]{1,0:T(8,128)(2,1)S(1)}, bf16[24,2048]{1,0:T(8,128)(2,1)}, u32[]{:S(2)}, u32[]{:S(2)}) %collective-permute-start.9) | collective-permute-done | bytes 98336 | tf_op jit(solution)/shard_map/ppermute | solution.py:25
  138.9 1.5 fusion.11
  140.4 0.1 fusion.14
  140.5 1.0 broadcast_in_dim.66
  141.5 3.5 %all-to-all-start.3 = ((bf16[8,24,2048]{2,1,0:T(8,128)(2,1)}), bf16[8,24,2048]{2,1,0:T(8,128)(2,1)S(1)}, u32[]{:S(2)}, u32[]{:S(2)}) async-start(bf16[8,24,2048]{2,1,0:T(8,128)(2,1)} %broadcast_in_dim.66), calls=%async_computation.3 | async-start | bytes 1572864 | tf_op jit(solution)/shard_map/all_to_all | solution.py:16
  145.1 0.8 fusion.3
  145.8 1.0 copy.69
  146.9 19.7 %all-to-all-done.3 = bf16[8,24,2048]{2,1,0:T(8,128)(2,1)S(1)} async-done(((bf16[8,24,2048]{2,1,0:T(8,128)(2,1)}), bf16[8,24,2048]{2,1,0:T(8,128)(2,1)S(1)}, u32[]{:S(2)}, u32[]{:S(2)}) %all-to-all-start.3) | async-done | bytes 786464 | tf_op jit(solution)/shard_map/all_to_all | solution.py:16
  166.6 0.9 copy-done.2
  167.5 7.1 %all-to-all-start.4 = ((bf16[8,256,256]{1,2,0:T(8,128)(2,1)}), bf16[8,256,256]{1,2,0:T(8,128)(2,1)S(1)}, u32[]{:S(2)}, u32[]{:S(2)}) async-start(bf16[8,256,256]{1,2,0:T(8,128)(2,1)} %bitcast.82), calls=%async_computation.4 | async-start | bytes 2097152 | tf_op jit(solution)/shard_map/all_to_all | solution.py:16
  174.6 1.9 collective-permute-start.15
  176.5 25.0 %all-to-all-done.4 = bf16[8,256,256]{1,2,0:T(8,128)(2,1)S(1)} async-done(((bf16[8,256,256]{1,2,0:T(8,128)(2,1)}), bf16[8,256,256]{1,2,0:T(8,128)(2,1)S(1)}, u32[]{:S(2)}, u32[]{:S(2)}) %all-to-all-start.4) | async-done | bytes 1048608 | tf_op jit(solution)/shard_map/all_to_all | solution.py:16
  201.5 0.1 reduce_sum.78
  201.7 0.1 copy.59
  201.8 15.3 %all_to_all.42 = bf16[8,32,256]{2,1,0:T(8,128)(2,1)S(1)} all-to-all(bf16[8,32,256]{2,1,0:T(8,128)(2,1)S(1)} %bitcast.93), channel_id=1, replica_groups=mesh['z'=8,'y'=8,'x'=8,'c'=2] {'y'}, dimensions={0} | all-to-all | bytes 262144 | tf_op jit(solution)/shard_map/all_to_all | solution.py:16
  217.2 10.1 %all_to_all.43 = f32[8,1,256]{2,1,0:T(1,128)S(1)} all-to-all(f32[8,1,256]{2,1,0:T(1,128)S(1)} %broadcast_in_dim.67), channel_id=1, replica_groups=mesh['z'=8,'y'=8,'x'=8,'c'=2] {'y'}, dimensions={0} | all-to-all | bytes 16384 | tf_op jit(solution)/shard_map/all_to_all | solution.py:16
  227.3 10.1 %all_to_all.44 = f32[8,1,256]{2,1,0:T(1,128)S(1)} all-to-all(f32[8,1,256]{2,1,0:T(1,128)S(1)} %broadcast_in_dim.68), channel_id=1, replica_groups=mesh['z'=8,'y'=8,'x'=8,'c'=2] {'z'}, dimensions={0} | all-to-all | bytes 16384 | tf_op jit(solution)/shard_map/all_to_all | solution.py:16
  237.4 0.6 reduce_sum.82
  238.0 0.2 broadcast_in_dim.53
  238.3 1.2 constant_dynamic-update-slice_fusion.1
  239.5 1.1 copy-done.7
  (47 shorter events, 0.4 us)
Async XLA Ops:
  0.6 87.1 %copy-start = (bf16[384,2048]{1,0:T(8,128)(2,1)S(1)}, bf16[384,2048]{1,0:T(8,128)(2,1)}, u32[]{:S(2)}) copy-start(bf16[384,2048]{1,0:T(8,128)(2,1)} %param.11) | copy-start | bytes 4718596
  0.6 44.6 %copy-start.1 = (bf16[384,2048]{1,0:T(8,128)(2,1)S(1)}, bf16[384,2048]{1,0:T(8,128)(2,1)}, u32[]{:S(2)}) copy-start(bf16[384,2048]{1,0:T(8,128)(2,1)} %param.6) | copy-start | bytes 4718596
  0.7 30.2 %copy-start.11 = (bf16[256,32]{0,1:T(8,128)(2,1)S(1)}, bf16[256,32]{0,1:T(8,128)(2,1)}, u32[]{:S(2)}) copy-start(bf16[256,32]{0,1:T(8,128)(2,1)} %param.10) | copy-start | bytes 49156
  0.7 44.6 %copy-start.10 = (f32[2048]{0:T(1024)S(1)}, f32[2048]{0:T(1024)}, u32[]{:S(2)}) copy-start(f32[2048]{0:T(1024)} %param.7) | copy-start | bytes 24580
  2.3 28.6 %all-to-all-start.2 = ((bf16[8,32,512]{2,1,0:T(8,128)(2,1)}), bf16[8,32,512]{2,1,0:T(8,128)(2,1)S(1)}, u32[]{:S(2)}, u32[]{:S(2)}) async-start(bf16[8,32,512]{2,1,0:T(8,128)(2,1)} %broadcast_in_dim.57), calls=%async_computation.2 | async-start | bytes 524288 | tf_op jit(solution)/shard_map/all_to_all | solution.py:16
  31.5 16.2 %all-to-all-start = ((bf16[8,32,256]{2,1,0:T(8,128)(2,1)}), bf16[8,32,256]{2,1,0:T(8,128)(2,1)S(1)}, u32[]{:S(2)}, u32[]{:S(2)}) async-start(bf16[8,32,256]{2,1,0:T(8,128)(2,1)} %broadcast_in_dim.54), calls=%async_computation | async-start | bytes 262144 | tf_op jit(solution)/shard_map/all_to_all | solution.py:16
  39.4 14.0 %collective-permute-start = (bf16[8,32,512]{2,1,0:T(8,128)(2,1)S(1)}, bf16[8,32,512]{2,1,0:T(8,128)(2,1)}, u32[]{:S(2)}, u32[]{:S(2)}) collective-permute-start(bf16[8,32,512]{2,1,0:T(8,128)(2,1)S(1)} %all-to-all-done.2), channel_id=1, source_target_pairs={{0,112},{16,0},{32,16},{48,32},{64,48},{80,64},{96,80},{112,96},{1... | collective-permute-start | bytes 786440 | tf_op jit(solution)/shard_map/ppermute | solution.py:25
  41.3 15.0 %collective-permute-start.1 = (bf16[8,32,512]{2,1,0:T(8,128)(2,1)S(1)}, bf16[8,32,512]{2,1,0:T(8,128)(2,1)}, u32[]{:S(2)}, u32[]{:S(2)}) collective-permute-start(bf16[8,32,512]{2,1,0:T(8,128)(2,1)S(1)} %all-to-all-done.2), channel_id=1, source_target_pairs={{0,16},{16,32},{32,48},{48,64},{64,80},{80,96},{96,112},{112,0},{1... | collective-permute-start | bytes 786440 | tf_op jit(solution)/shard_map/ppermute | solution.py:25
  48.9 38.8 %all-to-all-start.1 = ((bf16[8,8,32,256]{3,2,1,0:T(8,128)(2,1)}), bf16[8,8,32,256]{3,2,1,0:T(8,128)(2,1)}, u32[]{:S(2)}, u32[]{:S(2)}) async-start(bf16[8,8,32,256]{3,2,1,0:T(8,128)(2,1)} %broadcast_in_dim.55), calls=%async_computation.1 | async-start | bytes 2097152 | tf_op jit(solution)/shard_map/all_to_all | solution.py:16
  53.4 32.4 %copy-start.8 = (bf16[384,2048]{1,0:T(8,128)(2,1)S(1)}, bf16[384,2048]{1,0:T(8,128)(2,1)}, u32[]{:S(2)}) copy-start(bf16[384,2048]{1,0:T(8,128)(2,1)} %fusion.2) | copy-start | bytes 4718596
  53.4 8.6 %collective-permute-start.2 = (bf16[8,32,512]{2,1,0:T(8,128)(2,1)}, bf16[8,32,512]{2,1,0:T(8,128)(2,1)S(1)}, u32[]{:S(2)}, u32[]{:S(2)}) collective-permute-start(bf16[8,32,512]{2,1,0:T(8,128)(2,1)} %collective-permute-done), channel_id=1, source_target_pairs={{0,112},{16,0},{32,16},{48,32},{64,48},{80,64},{96,80},{112,96},{1... | collective-permute-start | bytes 786440 | tf_op jit(solution)/shard_map/ppermute | solution.py:25
  56.3 9.2 %collective-permute-start.3 = (bf16[8,32,512]{2,1,0:T(8,128)(2,1)}, bf16[8,32,512]{2,1,0:T(8,128)(2,1)S(1)}, u32[]{:S(2)}, u32[]{:S(2)}) collective-permute-start(bf16[8,32,512]{2,1,0:T(8,128)(2,1)} %collective-permute-done.1), channel_id=1, source_target_pairs={{0,16},{16,32},{32,48},{48,64},{64,80},{80,96},{96,112},{112,0},{1... | collective-permute-start | bytes 786440 | tf_op jit(solution)/shard_map/ppermute | solution.py:25
  62.0 14.9 %collective-permute-start.4 = (bf16[8,32,512]{2,1,0:T(8,128)(2,1)S(1)}, bf16[8,32,512]{2,1,0:T(8,128)(2,1)S(1)}, u32[]{:S(2)}, u32[]{:S(2)}) collective-permute-start(bf16[8,32,512]{2,1,0:T(8,128)(2,1)S(1)} %collective-permute-done.2), channel_id=1, source_target_pairs={{0,112},{16,0},{32,16},{48,32},{64,48},{80,64},{96,80},{112,96},{1... | collective-permute-start | bytes 786440 | tf_op jit(solution)/shard_map/ppermute | solution.py:25
  65.5 9.5 %collective-permute-start.5 = (bf16[8,32,512]{2,1,0:T(8,128)(2,1)S(1)}, bf16[8,32,512]{2,1,0:T(8,128)(2,1)S(1)}, u32[]{:S(2)}, u32[]{:S(2)}) collective-permute-start(bf16[8,32,512]{2,1,0:T(8,128)(2,1)S(1)} %collective-permute-done.3), channel_id=1, source_target_pairs={{0,16},{16,32},{32,48},{48,64},{64,80},{80,96},{96,112},{112,0},{1... | collective-permute-start | bytes 786440 | tf_op jit(solution)/shard_map/ppermute | solution.py:25
  75.0 9.5 %collective-permute-start.6 = (bf16[8,32,512]{2,1,0:T(8,128)(2,1)S(1)}, bf16[8,32,512]{2,1,0:T(8,128)(2,1)S(1)}, u32[]{:S(2)}, u32[]{:S(2)}) collective-permute-start(bf16[8,32,512]{2,1,0:T(8,128)(2,1)S(1)} %collective-permute-done.5), channel_id=1, source_target_pairs={{0,16},{16,32},{32,48},{48,64},{64,80},{80,96},{96,112},{112,0},{1... | collective-permute-start | bytes 786440 | tf_op jit(solution)/shard_map/ppermute | solution.py:25
  84.5 1.3 copy-start.4
  87.7 2.2 copy-start.5
  90.9 1.1 copy-start.6
  93.0 4.5 %collective-permute-start.7 = (bf16[192,2048]{1,0:T(8,128)(2,1)}, bf16[192,2048]{1,0:T(8,128)(2,1)}, u32[]{:S(2)}, u32[]{:S(2)}) collective-permute-start(bf16[192,2048]{1,0:T(8,128)(2,1)} %dynamic-slice_bitcast_fusion), channel_id=1, source_target_pairs={{0,1},{1,0},{2,3},{3,2},{4,5},{5,4},{6,7},{7,6},{8,9},{9,8},{10,11... | collective-permute-start | bytes 2359304 | tf_op jit(solution)/shard_map/ppermute | solution.py:29
  100.0 21.7 %collective-permute-start.10 = (bf16[24,2048]{1,0:T(8,128)(2,1)}, bf16[24,2048]{1,0:T(8,128)(2,1)}, u32[]{:S(2)}, u32[]{:S(2)}) collective-permute-start(bf16[24,2048]{1,0:T(8,128)(2,1)} %get-tuple-element.12), channel_id=1, source_target_pairs={{0,10},{2,12},{4,14},{6,0},{8,2},{10,4},{12,6},{14,8},{1,11},{3,13... | collective-permute-start | bytes 294920 | tf_op jit(solution)/shard_map/ppermute | solution.py:25
  106.5 18.5 %collective-permute-start.11 = (bf16[24,2048]{1,0:T(8,128)(2,1)}, bf16[24,2048]{1,0:T(8,128)(2,1)}, u32[]{:S(2)}, u32[]{:S(2)}) collective-permute-start(bf16[24,2048]{1,0:T(8,128)(2,1)} %get-tuple-element.11), channel_id=1, source_target_pairs={{0,4},{2,6},{4,8},{6,10},{8,12},{10,14},{12,0},{14,2},{1,5},{3,7},... | collective-permute-start | bytes 294920 | tf_op jit(solution)/shard_map/ppermute | solution.py:25
  109.2 19.6 %collective-permute-start.12 = (bf16[24,2048]{1,0:T(8,128)(2,1)}, bf16[24,2048]{1,0:T(8,128)(2,1)}, u32[]{:S(2)}, u32[]{:S(2)}) collective-permute-start(bf16[24,2048]{1,0:T(8,128)(2,1)} %get-tuple-element.10), channel_id=1, source_target_pairs={{0,12},{2,14},{4,0},{6,2},{8,4},{10,6},{12,8},{14,10},{1,13},{3,15... | collective-permute-start | bytes 294920 | tf_op jit(solution)/shard_map/ppermute | solution.py:25
  114.6 14.2 %collective-permute-start.13 = (bf16[24,2048]{1,0:T(8,128)(2,1)S(1)}, bf16[24,2048]{1,0:T(8,128)(2,1)}, u32[]{:S(2)}, u32[]{:S(2)}) collective-permute-start(bf16[24,2048]{1,0:T(8,128)(2,1)S(1)} %get-tuple-element.9), channel_id=1, source_target_pairs={{0,2},{2,4},{4,6},{6,8},{8,10},{10,12},{12,14},{14,0},{1,3},{3,5},... | collective-permute-start | bytes 294920 | tf_op jit(solution)/shard_map/ppermute | solution.py:25
  117.1 11.7 %collective-permute-start.14 = (bf16[24,2048]{1,0:T(8,128)(2,1)S(1)}, bf16[24,2048]{1,0:T(8,128)(2,1)}, u32[]{:S(2)}, u32[]{:S(2)}) collective-permute-start(bf16[24,2048]{1,0:T(8,128)(2,1)S(1)} %get-tuple-element.8), channel_id=1, source_target_pairs={{0,14},{2,0},{4,2},{6,4},{8,6},{10,8},{12,10},{14,12},{1,15},{3,1}... | collective-permute-start | bytes 294920 | tf_op jit(solution)/shard_map/ppermute | solution.py:25
  121.7 14.2 %collective-permute-start.8 = (bf16[24,2048]{1,0:T(8,128)(2,1)S(1)}, bf16[24,2048]{1,0:T(8,128)(2,1)}, u32[]{:S(2)}, u32[]{:S(2)}) collective-permute-start(bf16[24,2048]{1,0:T(8,128)(2,1)S(1)} %get-tuple-element.7), channel_id=1, source_target_pairs={{0,8},{2,10},{4,12},{6,14},{8,0},{10,2},{12,4},{14,6},{1,9},{3,11}... | collective-permute-start | bytes 294920 | tf_op jit(solution)/shard_map/ppermute | solution.py:25
  125.0 13.9 %collective-permute-start.9 = (bf16[24,2048]{1,0:T(8,128)(2,1)S(1)}, bf16[24,2048]{1,0:T(8,128)(2,1)}, u32[]{:S(2)}, u32[]{:S(2)}) collective-permute-start(bf16[24,2048]{1,0:T(8,128)(2,1)S(1)} %get-tuple-element.13), channel_id=1, source_target_pairs={{0,6},{2,8},{4,10},{6,12},{8,14},{10,0},{12,2},{14,4},{1,7},{3,9},... | collective-permute-start | bytes 294920 | tf_op jit(solution)/shard_map/ppermute | solution.py:25
  140.5 4.5 %copy-start.12 = (f32[384,512]{1,0:T(8,128)S(1)}, f32[384,512]{1,0:T(8,128)}, u32[]{:S(2)}) copy-start(f32[384,512]{1,0:T(8,128)} %fusion.35) | copy-start | bytes 2359300
  141.5 25.1 %all-to-all-start.3 = ((bf16[8,24,2048]{2,1,0:T(8,128)(2,1)}), bf16[8,24,2048]{2,1,0:T(8,128)(2,1)S(1)}, u32[]{:S(2)}, u32[]{:S(2)}) async-start(bf16[8,24,2048]{2,1,0:T(8,128)(2,1)} %broadcast_in_dim.66), calls=%async_computation.3 | async-start | bytes 1572864 | tf_op jit(solution)/shard_map/all_to_all | solution.py:16
  166.6 0.9 copy-start.2
  167.5 34.1 %all-to-all-start.4 = ((bf16[8,256,256]{1,2,0:T(8,128)(2,1)}), bf16[8,256,256]{1,2,0:T(8,128)(2,1)S(1)}, u32[]{:S(2)}, u32[]{:S(2)}) async-start(bf16[8,256,256]{1,2,0:T(8,128)(2,1)} %bitcast.82), calls=%async_computation.4 | async-start | bytes 2097152 | tf_op jit(solution)/shard_map/all_to_all | solution.py:16
  174.6 63.6 %collective-permute-start.15 = (bf16[1,192,2048]{2,1,0:T(8,128)(2,1)}, bf16[1,192,2048]{2,1,0:T(8,128)(2,1)}, u32[]{:S(2)}, u32[]{:S(2)}) collective-permute-start(bf16[1,192,2048]{2,1,0:T(8,128)(2,1)} %bitcast.84), channel_id=1, source_target_pairs={{0,1},{1,0},{2,3},{3,2},{4,5},{5,4},{6,7},{7,6},{8,9},{9,8},{10,11... | collective-permute-start | bytes 2359304 | tf_op jit(solution)/shard_map/ppermute | solution.py:29
  201.7 36.5 %copy-start.3 = (bf16[8,24,2048]{2,1,0:T(8,128)(2,1)S(1)}, bf16[8,24,2048]{2,1,0:T(8,128)(2,1)}, u32[]{:S(2)}) copy-start(bf16[8,24,2048]{2,1,0:T(8,128)(2,1)} %copy-done.2) | copy-start | bytes 2359300
  217.1 22.4 %copy-start.9 = (f32[32,256]{1,0:T(8,128)}, f32[32,256]{1,0:T(8,128)S(1)}, u32[]{:S(2)}) copy-start(f32[32,256]{1,0:T(8,128)S(1)} %convert_reduce_fusion) | copy-start | bytes 98308
  239.5 1.1 copy-start.7

commit v2 on v1

--- a/solution.py
+++ b/solution.py
@@ -58,10 +58,9 @@
     part_rows, units = w_gate.shape
     sizes = {a: lax.axis_size(a) for a in ("z", "y", "x", "c")}
 
-    down = copy_for_each(w_down.T, "y")
-    both = copy_for_each(jnp.concatenate([w_gate, w_up], axis=1), "z")
-    full_down = copy_for_each(down, "z").reshape(width, units)
-    both = ring(both, "y").reshape(width, 2 * units)
+    bundle = copy_for_each(jnp.concatenate([w_gate, w_up, w_down.T], axis=1), "z")
+    bundle = ring(bundle, "y").reshape(width, 3 * units)
+    both, full_down = bundle[:, : 2 * units], bundle[:, 2 * units :]
 
     xf = tokens.astype(f32)
     inv = lax.rsqrt(jnp.mean(xf * xf, axis=-1, keepdims=True) + EPS)
@@ -86,43 +85,59 @@
     d_both = jnp.concatenate([d_gate, d_up], axis=1)
     part = lax.dot_general(d_both, both, (((1,), (1,)), ((), ())), preferred_element_type=f32)
     core, place = lax.axis_index("c"), lax.axis_index("x")
-    pair = part.astype(bf16).reshape(sizes["c"], rows // sizes["c"], width)
-    theirs = lax.dynamic_index_in_dim(pair, 1 - core, 0, False)
-    theirs = exchange(theirs, "c", 1)
-    mine = lax.dynamic_index_in_dim(pair, core, 0, False)
-    own = mine.shape[0] // sizes["x"]
+    sign, peers = 1 - 2 * core, sizes["x"]
+    part = part.astype(bf16)
+    chip = rows // peers
+    own = chip // sizes["c"]
 
-    def piece(index):
-        start = (index % sizes["x"]) * own
-        return lax.dynamic_slice_in_dim(mine, start, own, 0).astype(
-            f32
-        ) + lax.dynamic_slice_in_dim(theirs, start, own, 0).astype(f32)
+    def rows_of(at, core_rows=None):
+        start = (at + peers) % peers * chip
+        if core_rows is None:
+            return lax.dynamic_slice_in_dim(part, start, chip, 0)
+        return lax.dynamic_slice_in_dim(part, start + core_rows * own, own, 0)
 
-    d_share = piece(place)
-    for by in (4, 3, 5, 2, 6, 1, 7):
-        got = shift(piece(place + by).astype(bf16), "x", by)
-        d_share = d_share + got.astype(f32)
+    near = range(1, peers // 2)
+    across = (place + peers // 2, place)
+    theirs = [rows_of(place - sign * j) for j in near] + [rows_of(a, 1 - core) for a in across]
+    mine = [rows_of(place + sign * j) for j in near] + [rows_of(a, core) for a in across]
+    theirs = exchange(jnp.concatenate(theirs, axis=0), "c", 1)
+    cuts = [chip * j for j in near] + [chip * len(near) + own]
+    theirs = jnp.split(theirs, cuts, axis=0)
+    sums = [a.astype(f32) + b.astype(f32) for a, b in zip(mine, theirs)]
+    d_share = sums[-1]
+    far = shift(sums[-2].astype(bf16), "x", peers // 2)
+    d_share = d_share + far.astype(f32)
+    arrived = jnp.zeros((chip, width), f32)
+    for j in reversed(near):
+        routes = [
+            (2 * x + c, 2 * ((x + (1 - 2 * c) * j) % peers) + c)
+            for x in range(peers)
+            for c in range(sizes["c"])
+        ]
+        arrived = arrived + lax.ppermute(sums[j - 1].astype(bf16), TP, routes).astype(f32)
+    d_share = d_share + lax.dynamic_slice_in_dim(arrived, core * own, own, 0)
+    arrived = lax.dynamic_slice_in_dim(arrived, (1 - core) * own, own, 0)
+    d_share = d_share + exchange(arrived.astype(bf16), "c", 1).astype(f32)
 
     along_y = jnp.sum(down_pieces.astype(f32), axis=0).astype(bf16)
     down_pieces = swap(along_y.reshape(sizes["y"], part_rows, units), "y")
     share = jnp.sum(down_pieces.astype(f32), axis=0)
     norms = jnp.sum(share * share, axis=0)
-    for axis in ("y", "z"):
-        norms = copy_for_each(norms, axis)
-        norms = jnp.sum(norms, axis=0)
+    norms = copy_for_each(norms, FS)
+    norms = jnp.sum(norms, axis=0)
 
-    offset = (core * sizes["x"] + place) * own
+    offset = (place * sizes["c"] + core) * own
     own_tokens = lax.dynamic_slice_in_dim(tokens, offset, own, 0).astype(f32)
     own_inv = lax.rsqrt(jnp.mean(own_tokens * own_tokens, axis=-1, keepdims=True) + EPS)
     scaled = own_tokens * own_inv
     d_scaled = d_share * norm_gain
     inner = jnp.mean(d_scaled * scaled, axis=-1, keepdims=True)
     grad_own = (own_inv * (d_scaled - scaled * inner)).astype(bf16)
-    grad_half = copy_for_each(grad_own, "x").reshape(1, -1, width)
+    grad_half = copy_for_each(grad_own, "x")[:, None]
     others = exchange(grad_half, "c", 1)
-    grad_tokens = jnp.zeros((sizes["c"], *grad_half.shape[1:]), bf16)
-    grad_tokens = lax.dynamic_update_slice(grad_tokens, grad_half, (core, 0, 0))
-    grad_tokens = lax.dynamic_update_slice(grad_tokens, others, (1 - core, 0, 0))
+    grad_tokens = jnp.zeros((peers, sizes["c"], own, width), bf16)
+    grad_tokens = lax.dynamic_update_slice(grad_tokens, grad_half, (0, core, 0, 0))
+    grad_tokens = lax.dynamic_update_slice(grad_tokens, others, (0, 1 - core, 0, 0))
     grad_tokens = grad_tokens.reshape(rows, width)
     return (grad_tokens, share.T, norms)
 

time: 242 us -> 202 us (0.83)
  blocking collectives: 35.5 us -> 0 us
  starting transfers between devices: 91.1 us -> 87.7 us
    all_to_all x3 -> x0, blocking collectives: 35.5 us -> none  [swap(): return lax.all_to_all(pieces, axis, split_axis=0, concat_axis=0, tiled=True)]
    ppermute x14 -> x8, starting transfers between devices: 47.8 us -> 24.9 us  [shift(): lax.ppermute(value, axis, [(i, (i + by) % peers) for i in range(peers)])]
    ppermute x0 -> x3, starting transfers between devices: none -> 12.4 us  [shards(): lax.ppermute(sums[j - 1].astype(bf16), TP, routes).astype(f32)]
    all_to_all x5, starting transfers between devices: 39.5 us -> 44.6 us  [swap(): return lax.all_to_all(pieces, axis, split_axis=0, concat_axis=0, tiled=True)]
    ppermute x0 -> x3, waiting for transfers between devices: none -> 4.78 us  [shards(): lax.ppermute(sums[j - 1].astype(bf16), TP, routes).astype(f32)]
    all_to_all x5, waiting for transfers between devices: 55.7 us -> 51.4 us  [swap(): return lax.all_to_all(pieces, axis, split_axis=0, concat_axis=0, tiled=True)]
    ppermute x14 -> x8, waiting for transfers between devices: 25.6 us -> 27.6 us  [shift(): lax.ppermute(value, axis, [(i, (i + by) % peers) for i in range(peers)])]
    ppermute x2 -> x3, starting transfers between devices: 3.82 us -> 5.73 us  [exchange(): lax.ppermute(value, axis, [(i, i ^ bit) for i in range(lax.axis_size(axis...]
  transfers between devices with their start and end apart: 21 -> 19, of which waited for: 11 -> 13; matrix products, arithmetic and copies ran while one was open for 5% -> 9% of each run, Pallas kernels for 0% -> 0%
where the time goes in v2:
time: 202 us; the launch traced here: 201 us
  starting transfers between devices  87.7 us (43%)
  waiting for transfers between devices  84.1 us (42%)
  local copies, waits for them, and re-layouts  12.8 us (6%)
  other arithmetic  11 us (5%)
  matrix products  4.51 us (2%)
    all_to_all x5, waiting for transfers between devices, swap(): return lax.all_to_all(pieces, axis, split_axis=0, concat_axis=0, tiled=True)  51.4 us
    all_to_all x5, starting transfers between devices, swap(): return lax.all_to_all(pieces, axis, split_axis=0, concat_axis=0, tiled=True)  44.6 us
    ppermute x8, waiting for transfers between devices, shift(): lax.ppermute(value, axis, [(i, (i + by) % peers) for i in range(peers)])  27.6 us
    ppermute x8, starting transfers between devices, shift(): lax.ppermute(value, axis, [(i, (i + by) % peers) for i in range(peers)])  24.9 us
    ppermute x3, starting transfers between devices, shards(): lax.ppermute(sums[j - 1].astype(bf16), TP, routes).astype(f32)  12.4 us
    ppermute x3, starting transfers between devices, exchange(): lax.ppermute(value, axis, [(i, i ^ bit) for i in range(lax.axis_size(axis...  5.73 us
    ppermute x3, waiting for transfers between devices, shards(): lax.ppermute(sums[j - 1].astype(bf16), TP, routes).astype(f32)  4.78 us
    unnamed x20, local copies, waits for them, and re-layouts  4.24 us
  transfers between devices with their start and end apart: 19, of which 13 were waited for; matrix products, arithmetic and copies ran while one was open for 9% of the time, Pallas kernels for 0%

profile of v2, /device:TPU:16, one launch (start us, length us, event | category | flops | bytes accessed | tf_op | source)
XLA Modules:
  0.0 201.2 jit_solution(4631195453586234268)
XLA Ops:
  0.7 0.9 pad_maximum_fusion
  1.6 0.8 broadcast_in_dim.49
  2.4 16.7 %all-to-all-start = ((bf16[8,32,768]{2,1,0:T(8,128)(2,1)}), bf16[8,32,768]{2,1,0:T(8,128)(2,1)S(1)}, u32[]{:S(2)}, u32[]{:S(2)}) async-start(bf16[8,32,768]{2,1,0:T(8,128)(2,1)} %broadcast_in_dim.49), calls=%async_computation | async-start | bytes 786432 | tf_op jit(solution)/shard_map/all_to_all | solution.py:16
  19.0 1.8 fusion
  20.8 12.9 %all-to-all-done = bf16[8,32,768]{2,1,0:T(8,128)(2,1)S(1)} async-done(((bf16[8,32,768]{2,1,0:T(8,128)(2,1)}), bf16[8,32,768]{2,1,0:T(8,128)(2,1)S(1)}, u32[]{:S(2)}, u32[]{:S(2)}) %all-to-all-start) | async-done | bytes 393248 | tf_op jit(solution)/shard_map/all_to_all | solution.py:16
  33.7 2.2 %collective-permute-start = (bf16[8,32,768]{2,1,0:T(8,128)(2,1)S(1)}, bf16[8,32,768]{2,1,0:T(8,128)(2,1)}, u32[]{:S(2)}, u32[]{:S(2)}) collective-permute-start(bf16[8,32,768]{2,1,0:T(8,128)(2,1)S(1)} %all-to-all-done), channel_id=1, source_target_pairs={{0,112},{16,0},{32,16},{48,32},{64,48},{80,64},{96,80},{112,96},{1... | collective-permute-start | bytes 1179656 | tf_op jit(solution)/shard_map/ppermute | solution.py:25
  36.0 3.6 %collective-permute-start.1 = (bf16[8,32,768]{2,1,0:T(8,128)(2,1)S(1)}, bf16[8,32,768]{2,1,0:T(8,128)(2,1)}, u32[]{:S(2)}, u32[]{:S(2)}) collective-permute-start(bf16[8,32,768]{2,1,0:T(8,128)(2,1)S(1)} %all-to-all-done), channel_id=1, source_target_pairs={{0,16},{16,32},{32,48},{48,64},{64,80},{80,96},{96,112},{112,0},{1... | collective-permute-start | bytes 1179656 | tf_op jit(solution)/shard_map/ppermute | solution.py:25
  39.6 1.6 fusion.2
  41.2 0.4 broadcast_in_dim.48
  41.6 4.3 %collective-permute-done = bf16[8,32,768]{2,1,0:T(8,128)(2,1)} collective-permute-done((bf16[8,32,768]{2,1,0:T(8,128)(2,1)S(1)}, bf16[8,32,768]{2,1,0:T(8,128)(2,1)}, u32[]{:S(2)}, u32[]{:S(2)}) %collective-permute-start) | collective-permute-done | bytes 393248 | tf_op jit(solution)/shard_map/ppermute | solution.py:25
  45.9 3.9 %collective-permute-start.2 = (bf16[8,32,768]{2,1,0:T(8,128)(2,1)}, bf16[8,32,768]{2,1,0:T(8,128)(2,1)S(1)}, u32[]{:S(2)}, u32[]{:S(2)}) collective-permute-start(bf16[8,32,768]{2,1,0:T(8,128)(2,1)} %collective-permute-done), channel_id=1, source_target_pairs={{0,112},{16,0},{32,16},{48,32},{64,48},{80,64},{96,80},{112,96},{1... | collective-permute-start | bytes 1179656 | tf_op jit(solution)/shard_map/ppermute | solution.py:25
  49.8 0.6 collective-permute-done.1
  50.4 1.9 collective-permute-start.3
  52.3 1.0 bitcast_dynamic-update-slice_fusion.5
  53.3 1.0 bitcast_dynamic-update-slice_fusion.4
  54.4 2.9 %collective-permute-done.2 = bf16[8,32,768]{2,1,0:T(8,128)(2,1)S(1)} collective-permute-done((bf16[8,32,768]{2,1,0:T(8,128)(2,1)}, bf16[8,32,768]{2,1,0:T(8,128)(2,1)S(1)}, u32[]{:S(2)}, u32[]{:S(2)}) %collective-permute-start.2) | collective-permute-done | bytes 393248 | tf_op jit(solution)/shard_map/ppermute | solution.py:25
  57.3 5.3 %collective-permute-start.4 = (bf16[8,32,768]{2,1,0:T(8,128)(2,1)S(1)}, bf16[8,32,768]{2,1,0:T(8,128)(2,1)S(1)}, u32[]{:S(2)}, u32[]{:S(2)}) collective-permute-start(bf16[8,32,768]{2,1,0:T(8,128)(2,1)S(1)} %collective-permute-done.2), channel_id=1, source_target_pairs={{0,112},{16,0},{32,16},{48,32},{64,48},{80,64},{96,80},{112,96},{1... | collective-permute-start | bytes 1179656 | tf_op jit(solution)/shard_map/ppermute | solution.py:25
  62.6 0.4 collective-permute-done.3
  63.0 1.9 collective-permute-start.5
  65.0 9.5 %collective-permute-done.5 = bf16[8,32,768]{2,1,0:T(8,128)(2,1)S(1)} collective-permute-done((bf16[8,32,768]{2,1,0:T(8,128)(2,1)S(1)}, bf16[8,32,768]{2,1,0:T(8,128)(2,1)S(1)}, u32[]{:S(2)}, u32[]{:S(2)}) %collective-permute-start.5) | collective-permute-done | bytes 393248 | tf_op jit(solution)/shard_map/ppermute | solution.py:25
  74.5 1.9 collective-permute-start.6
  76.5 8.6 %collective-permute-done.6 = bf16[8,32,768]{2,1,0:T(8,128)(2,1)S(1)} collective-permute-done((bf16[8,32,768]{2,1,0:T(8,128)(2,1)S(1)}, bf16[8,32,768]{2,1,0:T(8,128)(2,1)S(1)}, u32[]{:S(2)}, u32[]{:S(2)}) %collective-permute-start.6) | collective-permute-done | bytes 393248 | tf_op jit(solution)/shard_map/ppermute | solution.py:25
  85.2 1.0 fusion.5
  86.2 0.6 multiply_convert_fusion.1
  86.9 0.3 copy-done.7
  87.1 1.0 convolution_convert_fusion
  88.2 0.8 dynamic-slice_dynamic-update-slice_fusion.2
  88.9 0.7 dynamic-slice_dynamic-update-slice_fusion.1
  89.6 0.7 dynamic-slice_dynamic-update-slice_fusion
  90.3 0.6 dynamic-slice_dynamic-update-slice_fusion.4
  91.0 0.6 dynamic-slice_dynamic-update-slice_fusion.3
  91.6 1.9 collective-permute-start.7
  93.6 0.1 fusion.18
  93.7 1.9 fusion.3
  95.6 1.1 copy.67
  96.7 4.2 %all-to-all-start.2 = ((bf16[8,256,256]{1,2,0:T(8,128)(2,1)}), bf16[8,256,256]{1,2,0:T(8,128)(2,1)}, u32[]{:S(2)}, u32[]{:S(2)}) async-start(bf16[8,256,256]{1,2,0:T(8,128)(2,1)} %bitcast.55), calls=%async_computation.2 | async-start | bytes 2097152 | tf_op jit(solution)/shard_map/all_to_all | solution.py:16
  100.9 1.5 add_convert_fusion.2
  102.4 4.3 %collective-permute-start.10 = (bf16[48,2048]{1,0:T(8,128)(2,1)S(1)}, bf16[48,2048]{1,0:T(8,128)(2,1)S(1)}, u32[]{:S(2)}, u32[]{:S(2)}) collective-permute-start(bf16[48,2048]{1,0:T(8,128)(2,1)S(1)} %get-tuple-element.9), channel_id=1, source_target_pairs={{0,4},{1,13},{2,6},{3,15},{4,8},{5,1},{6,10},{7,3},{8,12},{9,5},{1... | collective-permute-start | bytes 589832 | tf_op jit(solution)/shard_map/ppermute | solution.py:117
  106.8 3.4 %collective-permute-start.11 = (bf16[48,2048]{1,0:T(8,128)(2,1)S(1)}, bf16[48,2048]{1,0:T(8,128)(2,1)S(1)}, u32[]{:S(2)}, u32[]{:S(2)}) collective-permute-start(bf16[48,2048]{1,0:T(8,128)(2,1)S(1)} %get-tuple-element.8), channel_id=1, source_target_pairs={{0,2},{1,15},{2,4},{3,1},{4,6},{5,3},{6,8},{7,5},{8,10},{9,7},{10,... | collective-permute-start | bytes 589832 | tf_op jit(solution)/shard_map/ppermute | solution.py:117
  110.2 4.7 %collective-permute-start.9 = (bf16[48,2048]{1,0:T(8,128)(2,1)S(1)}, bf16[48,2048]{1,0:T(8,128)(2,1)S(1)}, u32[]{:S(2)}, u32[]{:S(2)}) collective-permute-start(bf16[48,2048]{1,0:T(8,128)(2,1)S(1)} %get-tuple-element.7), channel_id=1, source_target_pairs={{0,6},{1,11},{2,8},{3,13},{4,10},{5,15},{6,12},{7,1},{8,14},{9,3},... | collective-permute-start | bytes 589832 | tf_op jit(solution)/shard_map/ppermute | solution.py:117
  114.9 1.6 add_convert_fusion.3
  116.5 4.1 %collective-permute-start.8 = (bf16[24,2048]{1,0:T(8,128)(2,1)}, bf16[24,2048]{1,0:T(8,128)(2,1)}, u32[]{:S(2)}, u32[]{:S(2)}) collective-permute-start(bf16[24,2048]{1,0:T(8,128)(2,1)} %add_convert_fusion.3), channel_id=1, source_target_pairs={{0,8},{2,10},{4,12},{6,14},{8,0},{10,2},{12,4},{14,6},{1,9},{3,11}... | collective-permute-start | bytes 294920 | tf_op jit(solution)/shard_map/ppermute | solution.py:25
  120.6 4.8 %collective-permute-done.9 = bf16[48,2048]{1,0:T(8,128)(2,1)S(1)} collective-permute-done((bf16[48,2048]{1,0:T(8,128)(2,1)S(1)}, bf16[48,2048]{1,0:T(8,128)(2,1)S(1)}, u32[]{:S(2)}, u32[]{:S(2)}) %collective-permute-start.9) | collective-permute-done | bytes 196640 | tf_op jit(solution)/shard_map/ppermute | solution.py:117
  125.5 0.7 dynamic-slice_convert_fusion
  126.2 1.9 collective-permute-start.12
  128.1 1.3 collective-permute-done.8
  129.4 0.3 collective-permute-done.12
  129.7 1.2 fusion.14
  130.9 0.1 fusion.17
  131.1 1.0 broadcast_in_dim.58
  132.0 7.7 %all-to-all-start.1 = ((bf16[8,24,2048]{2,1,0:T(8,128)(2,1)}), bf16[8,24,2048]{2,1,0:T(8,128)(2,1)S(1)}, u32[]{:S(2)}, u32[]{:S(2)}) async-start(bf16[8,24,2048]{2,1,0:T(8,128)(2,1)} %broadcast_in_dim.58), calls=%async_computation.1 | async-start | bytes 1572864 | tf_op jit(solution)/shard_map/all_to_all | solution.py:16
  139.8 1.4 reduce_sum.69
  141.1 0.8 copy.59
  141.9 21.3 %all-to-all-done.1 = bf16[8,24,2048]{2,1,0:T(8,128)(2,1)S(1)} async-done(((bf16[8,24,2048]{2,1,0:T(8,128)(2,1)}), bf16[8,24,2048]{2,1,0:T(8,128)(2,1)S(1)}, u32[]{:S(2)}, u32[]{:S(2)}) %all-to-all-start.1) | async-done | bytes 786464 | tf_op jit(solution)/shard_map/all_to_all | solution.py:16
  163.2 6.8 %all-to-all-start.3 = ((bf16[8,32,256]{2,1,0:T(8,128)(2,1)}), bf16[8,32,256]{2,1,0:T(8,128)(2,1)S(1)}, u32[]{:S(2)}, u32[]{:S(2)}) async-start(bf16[8,32,256]{2,1,0:T(8,128)(2,1)} %bitcast.21), calls=%async_computation.3 | async-start | bytes 262144 | tf_op jit(solution)/shard_map/all_to_all | solution.py:16
  170.0 1.9 collective-permute-start.13
  172.0 5.9 %all-to-all-done.3 = bf16[8,32,256]{2,1,0:T(8,128)(2,1)S(1)} async-done(((bf16[8,32,256]{2,1,0:T(8,128)(2,1)}), bf16[8,32,256]{2,1,0:T(8,128)(2,1)S(1)}, u32[]{:S(2)}, u32[]{:S(2)}) %all-to-all-start.3) | async-done | bytes 131104 | tf_op jit(solution)/shard_map/all_to_all | solution.py:16
  177.9 0.7 broadcast_in_dim.60
  178.6 9.1 %all-to-all-start.4 = ((f32[64,1,256]{2,1,0:T(1,128)}), f32[64,1,256]{2,1,0:T(1,128)S(1)}, u32[]{:S(2)}, u32[]{:S(2)}) async-start(f32[64,1,256]{2,1,0:T(1,128)} %broadcast_in_dim.60), calls=%async_computation.4 | async-start | bytes 131072 | tf_op jit(solution)/shard_map/all_to_all | solution.py:16
  187.7 11.4 %all-to-all-done.4 = f32[64,1,256]{2,1,0:T(1,128)S(1)} async-done(((f32[64,1,256]{2,1,0:T(1,128)}), f32[64,1,256]{2,1,0:T(1,128)S(1)}, u32[]{:S(2)}, u32[]{:S(2)}) %all-to-all-start.4) | async-done | bytes 65568 | tf_op jit(solution)/shard_map/all_to_all | solution.py:16
  199.0 0.7 reduce_sum.72
  199.7 0.2 broadcast_in_dim.47
  199.9 0.1 constant_dynamic-update-slice_fusion
  200.1 1.1 copy-done.3
  (34 shorter events, 0.5 us)
Async XLA Ops:
  0.6 85.6 %copy-start = (bf16[384,2048]{1,0:T(8,128)(2,1)S(1)}, bf16[384,2048]{1,0:T(8,128)(2,1)}, u32[]{:S(2)}) copy-start(bf16[384,2048]{1,0:T(8,128)(2,1)} %param.11) | copy-start | bytes 4718596
  0.6 38.9 %copy-start.1 = (bf16[384,2048]{1,0:T(8,128)(2,1)S(1)}, bf16[384,2048]{1,0:T(8,128)(2,1)}, u32[]{:S(2)}) copy-start(bf16[384,2048]{1,0:T(8,128)(2,1)} %param.6) | copy-start | bytes 4718596
  0.7 38.9 %copy-start.6 = (f32[2048]{0:T(1024)S(1)}, f32[2048]{0:T(1024)}, u32[]{:S(2)}) copy-start(f32[2048]{0:T(1024)} %param.7) | copy-start | bytes 24580
  2.4 31.4 %all-to-all-start = ((bf16[8,32,768]{2,1,0:T(8,128)(2,1)}), bf16[8,32,768]{2,1,0:T(8,128)(2,1)S(1)}, u32[]{:S(2)}, u32[]{:S(2)}) async-start(bf16[8,32,768]{2,1,0:T(8,128)(2,1)} %broadcast_in_dim.49), calls=%async_computation | async-start | bytes 786432 | tf_op jit(solution)/shard_map/all_to_all | solution.py:16
  33.7 12.1 %collective-permute-start = (bf16[8,32,768]{2,1,0:T(8,128)(2,1)S(1)}, bf16[8,32,768]{2,1,0:T(8,128)(2,1)}, u32[]{:S(2)}, u32[]{:S(2)}) collective-permute-start(bf16[8,32,768]{2,1,0:T(8,128)(2,1)S(1)} %all-to-all-done), channel_id=1, source_target_pairs={{0,112},{16,0},{32,16},{48,32},{64,48},{80,64},{96,80},{112,96},{1... | collective-permute-start | bytes 1179656 | tf_op jit(solution)/shard_map/ppermute | solution.py:25
  36.0 14.4 %collective-permute-start.1 = (bf16[8,32,768]{2,1,0:T(8,128)(2,1)S(1)}, bf16[8,32,768]{2,1,0:T(8,128)(2,1)}, u32[]{:S(2)}, u32[]{:S(2)}) collective-permute-start(bf16[8,32,768]{2,1,0:T(8,128)(2,1)S(1)} %all-to-all-done), channel_id=1, source_target_pairs={{0,16},{16,32},{32,48},{48,64},{64,80},{80,96},{96,112},{112,0},{1... | collective-permute-start | bytes 1179656 | tf_op jit(solution)/shard_map/ppermute | solution.py:25
  45.9 11.4 %collective-permute-start.2 = (bf16[8,32,768]{2,1,0:T(8,128)(2,1)}, bf16[8,32,768]{2,1,0:T(8,128)(2,1)S(1)}, u32[]{:S(2)}, u32[]{:S(2)}) collective-permute-start(bf16[8,32,768]{2,1,0:T(8,128)(2,1)} %collective-permute-done), channel_id=1, source_target_pairs={{0,112},{16,0},{32,16},{48,32},{64,48},{80,64},{96,80},{112,96},{1... | collective-permute-start | bytes 1179656 | tf_op jit(solution)/shard_map/ppermute | solution.py:25
  50.4 12.6 %collective-permute-start.3 = (bf16[8,32,768]{2,1,0:T(8,128)(2,1)}, bf16[8,32,768]{2,1,0:T(8,128)(2,1)S(1)}, u32[]{:S(2)}, u32[]{:S(2)}) collective-permute-start(bf16[8,32,768]{2,1,0:T(8,128)(2,1)} %collective-permute-done.1), channel_id=1, source_target_pairs={{0,16},{16,32},{32,48},{48,64},{64,80},{80,96},{96,112},{112,0},{1... | collective-permute-start | bytes 1179656 | tf_op jit(solution)/shard_map/ppermute | solution.py:25
  57.3 19.2 %collective-permute-start.4 = (bf16[8,32,768]{2,1,0:T(8,128)(2,1)S(1)}, bf16[8,32,768]{2,1,0:T(8,128)(2,1)S(1)}, u32[]{:S(2)}, u32[]{:S(2)}) collective-permute-start(bf16[8,32,768]{2,1,0:T(8,128)(2,1)S(1)} %collective-permute-done.2), channel_id=1, source_target_pairs={{0,112},{16,0},{32,16},{48,32},{64,48},{80,64},{96,80},{112,96},{1... | collective-permute-start | bytes 1179656 | tf_op jit(solution)/shard_map/ppermute | solution.py:25
  63.0 11.5 %collective-permute-start.5 = (bf16[8,32,768]{2,1,0:T(8,128)(2,1)S(1)}, bf16[8,32,768]{2,1,0:T(8,128)(2,1)S(1)}, u32[]{:S(2)}, u32[]{:S(2)}) collective-permute-start(bf16[8,32,768]{2,1,0:T(8,128)(2,1)S(1)} %collective-permute-done.3), channel_id=1, source_target_pairs={{0,16},{16,32},{32,48},{48,64},{64,80},{80,96},{96,112},{112,0},{1... | collective-permute-start | bytes 1179656 | tf_op jit(solution)/shard_map/ppermute | solution.py:25
  65.0 20.2 %copy-start.4 = (bf16[384,2048]{1,0:T(8,128)(2,1)S(1)}, bf16[384,2048]{1,0:T(8,128)(2,1)}, u32[]{:S(2)}) copy-start(bf16[384,2048]{1,0:T(8,128)(2,1)} %fusion.2) | copy-start | bytes 4718596
  74.5 10.6 %collective-permute-start.6 = (bf16[8,32,768]{2,1,0:T(8,128)(2,1)S(1)}, bf16[8,32,768]{2,1,0:T(8,128)(2,1)S(1)}, u32[]{:S(2)}, u32[]{:S(2)}) collective-permute-start(bf16[8,32,768]{2,1,0:T(8,128)(2,1)S(1)} %collective-permute-done.5), channel_id=1, source_target_pairs={{0,16},{16,32},{32,48},{48,64},{64,80},{80,96},{96,112},{112,0},{1... | collective-permute-start | bytes 1179656 | tf_op jit(solution)/shard_map/ppermute | solution.py:25
  86.2 0.9 copy-start.7
  88.2 2.8 %copy-start.2 = (bf16[384,2048]{1,0:T(8,128)(2,1)}, bf16[384,2048]{1,0:T(8,128)(2,1)S(1)}, u32[]{:S(2)}) copy-start(bf16[384,2048]{1,0:T(8,128)(2,1)S(1)} %convolution_convert_fusion) | copy-start | bytes 4718596
  91.6 9.3 %collective-permute-start.7 = (bf16[192,2048]{1,0:T(8,128)(2,1)}, bf16[192,2048]{1,0:T(8,128)(2,1)}, u32[]{:S(2)}, u32[]{:S(2)}) collective-permute-start(bf16[192,2048]{1,0:T(8,128)(2,1)} %dynamic-slice_dynamic-update-slice_fusion.3), channel_id=1, source_target_pairs={{0,1},{1,0},{2,3},{3,2},{4,5},{5,4},{6,7},{7,6},{8,9},{9,8},{10,11... | collective-permute-start | bytes 2359304 | tf_op jit(solution)/shard_map/ppermute | solution.py:29
  96.7 34.4 %all-to-all-start.2 = ((bf16[8,256,256]{1,2,0:T(8,128)(2,1)}), bf16[8,256,256]{1,2,0:T(8,128)(2,1)}, u32[]{:S(2)}, u32[]{:S(2)}) async-start(bf16[8,256,256]{1,2,0:T(8,128)(2,1)} %bitcast.55), calls=%async_computation.2 | async-start | bytes 2097152 | tf_op jit(solution)/shard_map/all_to_all | solution.py:16
  102.4 18.2 %collective-permute-start.10 = (bf16[48,2048]{1,0:T(8,128)(2,1)S(1)}, bf16[48,2048]{1,0:T(8,128)(2,1)S(1)}, u32[]{:S(2)}, u32[]{:S(2)}) collective-permute-start(bf16[48,2048]{1,0:T(8,128)(2,1)S(1)} %get-tuple-element.9), channel_id=1, source_target_pairs={{0,4},{1,13},{2,6},{3,15},{4,8},{5,1},{6,10},{7,3},{8,12},{9,5},{1... | collective-permute-start | bytes 589832 | tf_op jit(solution)/shard_map/ppermute | solution.py:117
  106.8 13.9 %collective-permute-start.11 = (bf16[48,2048]{1,0:T(8,128)(2,1)S(1)}, bf16[48,2048]{1,0:T(8,128)(2,1)S(1)}, u32[]{:S(2)}, u32[]{:S(2)}) collective-permute-start(bf16[48,2048]{1,0:T(8,128)(2,1)S(1)} %get-tuple-element.8), channel_id=1, source_target_pairs={{0,2},{1,15},{2,4},{3,1},{4,6},{5,3},{6,8},{7,5},{8,10},{9,7},{10,... | collective-permute-start | bytes 589832 | tf_op jit(solution)/shard_map/ppermute | solution.py:117
  110.2 15.2 %collective-permute-start.9 = (bf16[48,2048]{1,0:T(8,128)(2,1)S(1)}, bf16[48,2048]{1,0:T(8,128)(2,1)S(1)}, u32[]{:S(2)}, u32[]{:S(2)}) collective-permute-start(bf16[48,2048]{1,0:T(8,128)(2,1)S(1)} %get-tuple-element.7), channel_id=1, source_target_pairs={{0,6},{1,11},{2,8},{3,13},{4,10},{5,15},{6,12},{7,1},{8,14},{9,3},... | collective-permute-start | bytes 589832 | tf_op jit(solution)/shard_map/ppermute | solution.py:117
  116.5 13.0 %collective-permute-start.8 = (bf16[24,2048]{1,0:T(8,128)(2,1)}, bf16[24,2048]{1,0:T(8,128)(2,1)}, u32[]{:S(2)}, u32[]{:S(2)}) collective-permute-start(bf16[24,2048]{1,0:T(8,128)(2,1)} %add_convert_fusion.3), channel_id=1, source_target_pairs={{0,8},{2,10},{4,12},{6,14},{8,0},{10,2},{12,4},{14,6},{1,9},{3,11}... | collective-permute-start | bytes 294920 | tf_op jit(solution)/shard_map/ppermute | solution.py:25
  126.2 3.5 %collective-permute-start.12 = (bf16[24,2048]{1,0:T(8,128)(2,1)}, bf16[24,2048]{1,0:T(8,128)(2,1)}, u32[]{:S(2)}, u32[]{:S(2)}) collective-permute-start(bf16[24,2048]{1,0:T(8,128)(2,1)} %dynamic-slice_convert_fusion), channel_id=1, source_target_pairs={{0,1},{1,0},{2,3},{3,2},{4,5},{5,4},{6,7},{7,6},{8,9},{9,8},{10,11... | collective-permute-start | bytes 294920 | tf_op jit(solution)/shard_map/ppermute | solution.py:29
  132.0 31.2 %all-to-all-start.1 = ((bf16[8,24,2048]{2,1,0:T(8,128)(2,1)}), bf16[8,24,2048]{2,1,0:T(8,128)(2,1)S(1)}, u32[]{:S(2)}, u32[]{:S(2)}) async-start(bf16[8,24,2048]{2,1,0:T(8,128)(2,1)} %broadcast_in_dim.58), calls=%async_computation.1 | async-start | bytes 1572864 | tf_op jit(solution)/shard_map/all_to_all | solution.py:16
  163.2 14.6 %all-to-all-start.3 = ((bf16[8,32,256]{2,1,0:T(8,128)(2,1)}), bf16[8,32,256]{2,1,0:T(8,128)(2,1)S(1)}, u32[]{:S(2)}, u32[]{:S(2)}) async-start(bf16[8,32,256]{2,1,0:T(8,128)(2,1)} %bitcast.21), calls=%async_computation.3 | async-start | bytes 262144 | tf_op jit(solution)/shard_map/all_to_all | solution.py:16
  170.0 29.9 %collective-permute-start.13 = (bf16[8,1,24,2048]{3,2,1,0:T(8,128)(2,1)S(1)}, bf16[8,1,24,2048]{3,2,1,0:T(8,128)(2,1)S(1)}, u32[]{:S(2)}, u32[]{:S(2)}) collective-permute-start(bf16[8,1,24,2048]{3,2,1,0:T(8,128)(2,1)S(1)} %bitcast.56), channel_id=1, source_target_pairs={{0,1},{1,0},{2,3},{3,2},{4,5},{5,4},{6,7},{7,6},{8,9},{9,8},{10,11... | collective-permute-start | bytes 2359304 | tf_op jit(solution)/shard_map/ppermute | solution.py:29
  177.9 22.2 %copy-start.5 = (f32[32,256]{1,0:T(8,128)}, f32[32,256]{1,0:T(8,128)S(1)}, u32[]{:S(2)}) copy-start(f32[32,256]{1,0:T(8,128)S(1)} %convert_reduce_fusion) | copy-start | bytes 98308
  178.6 20.5 %all-to-all-start.4 = ((f32[64,1,256]{2,1,0:T(1,128)}), f32[64,1,256]{2,1,0:T(1,128)S(1)}, u32[]{:S(2)}, u32[]{:S(2)}) async-start(f32[64,1,256]{2,1,0:T(1,128)} %broadcast_in_dim.60), calls=%async_computation.4 | async-start | bytes 131072 | tf_op jit(solution)/shard_map/all_to_all | solution.py:16
  200.1 1.1 copy-start.3

commit v3 on v2

--- a/solution.py
+++ b/solution.py
@@ -107,24 +107,28 @@
     d_share = sums[-1]
     far = shift(sums[-2].astype(bf16), "x", peers // 2)
     d_share = d_share + far.astype(f32)
-    arrived = jnp.zeros((chip, width), f32)
+    arrived = []
     for j in reversed(near):
         routes = [
             (2 * x + c, 2 * ((x + (1 - 2 * c) * j) % peers) + c)
             for x in range(peers)
             for c in range(sizes["c"])
         ]
-        arrived = arrived + lax.ppermute(sums[j - 1].astype(bf16), TP, routes).astype(f32)
+        arrived.append(lax.ppermute(sums[j - 1].astype(bf16), TP, routes))
+    along_y = jnp.sum(down_pieces.astype(f32), axis=0).astype(bf16)
+    down_pieces = copy_for_each(along_y, "y")
+    *arrived, _ = lax.optimization_barrier((*arrived, along_y))
+    arrived = sum(a.astype(f32) for a in arrived)
     d_share = d_share + lax.dynamic_slice_in_dim(arrived, core * own, own, 0)
     arrived = lax.dynamic_slice_in_dim(arrived, (1 - core) * own, own, 0)
     d_share = d_share + exchange(arrived.astype(bf16), "c", 1).astype(f32)
 
-    along_y = jnp.sum(down_pieces.astype(f32), axis=0).astype(bf16)
-    down_pieces = swap(along_y.reshape(sizes["y"], part_rows, units), "y")
-    share = jnp.sum(down_pieces.astype(f32), axis=0)
-    norms = jnp.sum(share * share, axis=0)
-    norms = copy_for_each(norms, FS)
-    norms = jnp.sum(norms, axis=0)
+    block = jnp.sum(down_pieces.astype(f32), axis=0)
+    share = lax.dynamic_slice_in_dim(block, lax.axis_index("y") * part_rows, part_rows, 0)
+    norms = jnp.sum(block * block, axis=0)
+    for bit in (1, 2, 4):
+        others = exchange(norms, "z", bit)
+        norms = norms + others
 
     offset = (place * sizes["c"] + core) * own
     own_tokens = lax.dynamic_slice_in_dim(tokens, offset, own, 0).astype(f32)

time: 202 us -> 230 us (1.14)
  waiting for transfers between devices: 84.1 us -> 101 us
  starting transfers between devices: 87.7 us -> 92.9 us
  local copies, waits for them, and re-layouts: 12.8 us -> 15.6 us
  other arithmetic: 11 us -> 13.5 us
    ppermute x3 -> x6, starting transfers between devices: 5.73 us -> 22.1 us  [exchange(): lax.ppermute(value, axis, [(i, i ^ bit) for i in range(lax.axis_size(axis...]
    all_to_all x5 -> x4, starting transfers between devices: 44.6 us -> 33.5 us  [swap(): return lax.all_to_all(pieces, axis, split_axis=0, concat_axis=0, tiled=True)]
    all_to_all x5 -> x4, waiting for transfers between devices: 51.4 us -> 61.9 us  [swap(): return lax.all_to_all(pieces, axis, split_axis=0, concat_axis=0, tiled=True)]
    ppermute x3 -> x6, waiting for transfers between devices: 0.26 us -> 8 us  [exchange(): lax.ppermute(value, axis, [(i, i ^ bit) for i in range(lax.axis_size(axis...]
  transfers between devices with their start and end apart: 19 -> 21, of which waited for: 13 -> 15; matrix products, arithmetic and copies ran while one was open for 9% -> 10% of each run, Pallas kernels for 0% -> 0%
where the time goes in v3:
time: 230 us; the launch traced here: 229 us
  waiting for transfers between devices  101 us (44%)
  starting transfers between devices  92.9 us (40%)
  local copies, waits for them, and re-layouts  15.6 us (7%)
  other arithmetic  13.5 us (6%)
  matrix products  4.98 us (2%)
    all_to_all x4, waiting for transfers between devices, swap(): return lax.all_to_all(pieces, axis, split_axis=0, concat_axis=0, tiled=True)  61.9 us
    all_to_all x4, starting transfers between devices, swap(): return lax.all_to_all(pieces, axis, split_axis=0, concat_axis=0, tiled=True)  33.5 us
    ppermute x8, waiting for transfers between devices, shift(): lax.ppermute(value, axis, [(i, (i + by) % peers) for i in range(peers)])  26.3 us
    ppermute x8, starting transfers between devices, shift(): lax.ppermute(value, axis, [(i, (i + by) % peers) for i in range(peers)])  24.9 us
    ppermute x6, starting transfers between devices, exchange(): lax.ppermute(value, axis, [(i, i ^ bit) for i in range(lax.axis_size(axis...  22.1 us
    ppermute x3, starting transfers between devices, shards(): arrived.append(lax.ppermute(sums[j - 1].astype(bf16), TP, routes))  12.4 us
    ppermute x6, waiting for transfers between devices, exchange(): lax.ppermute(value, axis, [(i, i ^ bit) for i in range(lax.axis_size(axis...  8 us
    ppermute x3, waiting for transfers between devices, shards(): arrived.append(lax.ppermute(sums[j - 1].astype(bf16), TP, routes))  4.86 us
  transfers between devices with their start and end apart: 21, of which 15 were waited for; matrix products, arithmetic and copies ran while one was open for 10% of the time, Pallas kernels for 0%

profile of v3, /device:TPU:16, one launch (start us, length us, event | category | flops | bytes accessed | tf_op | source)
XLA Modules:
  0.0 229.2 jit_solution(9370396059779666130)
XLA Ops:
  0.7 0.9 pad_maximum_fusion
  1.6 0.8 broadcast_in_dim.49
  2.4 16.7 %all-to-all-start = ((bf16[8,32,768]{2,1,0:T(8,128)(2,1)}), bf16[8,32,768]{2,1,0:T(8,128)(2,1)S(1)}, u32[]{:S(2)}, u32[]{:S(2)}) async-start(bf16[8,32,768]{2,1,0:T(8,128)(2,1)} %broadcast_in_dim.49), calls=%async_computation | async-start | bytes 786432 | tf_op jit(solution)/shard_map/all_to_all | solution.py:16
  19.0 1.8 fusion
  20.8 12.9 %all-to-all-done = bf16[8,32,768]{2,1,0:T(8,128)(2,1)S(1)} async-done(((bf16[8,32,768]{2,1,0:T(8,128)(2,1)}), bf16[8,32,768]{2,1,0:T(8,128)(2,1)S(1)}, u32[]{:S(2)}, u32[]{:S(2)}) %all-to-all-start) | async-done | bytes 393248 | tf_op jit(solution)/shard_map/all_to_all | solution.py:16
  33.7 2.2 collective-permute-start
  36.0 3.6 %collective-permute-start.1 = (bf16[8,32,768]{2,1,0:T(8,128)(2,1)S(1)}, bf16[8,32,768]{2,1,0:T(8,128)(2,1)}, u32[]{:S(2)}, u32[]{:S(2)}) collective-permute-start(bf16[8,32,768]{2,1,0:T(8,128)(2,1)S(1)} %all-to-all-done), channel_id=1, source_target_pairs={{0,16},{16,32},{32,48},{48,64},{64,80},{80,96},{96,112},{112,0},{1... | collective-permute-start | bytes 1179656 | tf_op jit(solution)/shard_map/ppermute | solution.py:25
  39.6 1.6 fusion.2
  41.6 4.3 %collective-permute-done = bf16[8,32,768]{2,1,0:T(8,128)(2,1)} collective-permute-done((bf16[8,32,768]{2,1,0:T(8,128)(2,1)S(1)}, bf16[8,32,768]{2,1,0:T(8,128)(2,1)}, u32[]{:S(2)}, u32[]{:S(2)}) %collective-permute-start) | collective-permute-done | bytes 393248 | tf_op jit(solution)/shard_map/ppermute | solution.py:25
  45.9 3.9 %collective-permute-start.2 = (bf16[8,32,768]{2,1,0:T(8,128)(2,1)}, bf16[8,32,768]{2,1,0:T(8,128)(2,1)S(1)}, u32[]{:S(2)}, u32[]{:S(2)}) collective-permute-start(bf16[8,32,768]{2,1,0:T(8,128)(2,1)} %collective-permute-done), channel_id=1, source_target_pairs={{0,112},{16,0},{32,16},{48,32},{64,48},{80,64},{96,80},{112,96},{1... | collective-permute-start | bytes 1179656 | tf_op jit(solution)/shard_map/ppermute | solution.py:25
  49.8 0.6 collective-permute-done.1
  50.4 1.9 collective-permute-start.3
  52.3 1.0 bitcast_dynamic-update-slice_fusion.5
  53.3 1.0 bitcast_dynamic-update-slice_fusion.4
  54.4 2.9 %collective-permute-done.2 = bf16[8,32,768]{2,1,0:T(8,128)(2,1)S(1)} collective-permute-done((bf16[8,32,768]{2,1,0:T(8,128)(2,1)}, bf16[8,32,768]{2,1,0:T(8,128)(2,1)S(1)}, u32[]{:S(2)}, u32[]{:S(2)}) %collective-permute-start.2) | collective-permute-done | bytes 393248 | tf_op jit(solution)/shard_map/ppermute | solution.py:25
  57.3 5.3 %collective-permute-start.4 = (bf16[8,32,768]{2,1,0:T(8,128)(2,1)S(1)}, bf16[8,32,768]{2,1,0:T(8,128)(2,1)S(1)}, u32[]{:S(2)}, u32[]{:S(2)}) collective-permute-start(bf16[8,32,768]{2,1,0:T(8,128)(2,1)S(1)} %collective-permute-done.2), channel_id=1, source_target_pairs={{0,112},{16,0},{32,16},{48,32},{64,48},{80,64},{96,80},{112,96},{1... | collective-permute-start | bytes 1179656 | tf_op jit(solution)/shard_map/ppermute | solution.py:25
  63.0 1.9 collective-permute-start.5
  65.0 9.5 %collective-permute-done.5 = bf16[8,32,768]{2,1,0:T(8,128)(2,1)S(1)} collective-permute-done((bf16[8,32,768]{2,1,0:T(8,128)(2,1)S(1)}, bf16[8,32,768]{2,1,0:T(8,128)(2,1)S(1)}, u32[]{:S(2)}, u32[]{:S(2)}) %collective-permute-start.5) | collective-permute-done | bytes 393248 | tf_op jit(solution)/shard_map/ppermute | solution.py:25
  74.5 1.9 collective-permute-start.6
  76.5 8.6 %collective-permute-done.6 = bf16[8,32,768]{2,1,0:T(8,128)(2,1)S(1)} collective-permute-done((bf16[8,32,768]{2,1,0:T(8,128)(2,1)S(1)}, bf16[8,32,768]{2,1,0:T(8,128)(2,1)S(1)}, u32[]{:S(2)}, u32[]{:S(2)}) %collective-permute-start.6) | collective-permute-done | bytes 393248 | tf_op jit(solution)/shard_map/ppermute | solution.py:25
  85.1 1.1 slice.16
  86.3 1.0 fusion.5
  87.3 0.8 fusion.3
  88.2 1.1 copy.44
  89.3 4.2 %all-to-all-start.1 = ((bf16[8,256,256]{1,2,0:T(8,128)(2,1)}), bf16[8,256,256]{1,2,0:T(8,128)(2,1)}, u32[]{:S(2)}, u32[]{:S(2)}) async-start(bf16[8,256,256]{1,2,0:T(8,128)(2,1)} %bitcast.55), calls=%async_computation.1 | async-start | bytes 2097152 | tf_op jit(solution)/shard_map/all_to_all | solution.py:16
  93.5 2.2 multiply_convert_fusion.1
  95.9 1.0 convolution_convert_fusion
  97.0 0.7 dynamic-slice_dynamic-update-slice_fusion.2
  97.7 0.7 dynamic-slice_dynamic-update-slice_fusion.1
  98.4 0.7 dynamic-slice_dynamic-update-slice_fusion
  99.1 0.7 dynamic-slice_dynamic-update-slice_fusion.4
  99.8 0.6 dynamic-slice_dynamic-update-slice_fusion.3
  100.4 1.9 collective-permute-start.7
  102.5 2.4 %collective-permute-done.7 = bf16[192,2048]{1,0:T(8,128)(2,1)} collective-permute-done((bf16[192,2048]{1,0:T(8,128)(2,1)}, bf16[192,2048]{1,0:T(8,128)(2,1)}, u32[]{:S(2)}, u32[]{:S(2)}) %collective-permute-start.7) | collective-permute-done | bytes 786464 | tf_op jit(solution)/shard_map/ppermute | solution.py:29
  104.9 2.2 add_convert_fusion
  107.1 4.3 %collective-permute-start.10 = (bf16[48,2048]{1,0:T(8,128)(2,1)}, bf16[48,2048]{1,0:T(8,128)(2,1)}, u32[]{:S(2)}, u32[]{:S(2)}) collective-permute-start(bf16[48,2048]{1,0:T(8,128)(2,1)} %get-tuple-element.14), channel_id=1, source_target_pairs={{0,4},{1,13},{2,6},{3,15},{4,8},{5,1},{6,10},{7,3},{8,12},{9,5},{1... | collective-permute-start | bytes 589832 | tf_op jit(solution)/shard_map/ppermute | solution.py:117
  111.4 3.4 %collective-permute-start.11 = (bf16[48,2048]{1,0:T(8,128)(2,1)S(1)}, bf16[48,2048]{1,0:T(8,128)(2,1)}, u32[]{:S(2)}, u32[]{:S(2)}) collective-permute-start(bf16[48,2048]{1,0:T(8,128)(2,1)S(1)} %get-tuple-element.13), channel_id=1, source_target_pairs={{0,2},{1,15},{2,4},{3,1},{4,6},{5,3},{6,8},{7,5},{8,10},{9,7},{10,... | collective-permute-start | bytes 589832 | tf_op jit(solution)/shard_map/ppermute | solution.py:117
  114.8 4.7 %collective-permute-start.9 = (bf16[48,2048]{1,0:T(8,128)(2,1)S(1)}, bf16[48,2048]{1,0:T(8,128)(2,1)}, u32[]{:S(2)}, u32[]{:S(2)}) collective-permute-start(bf16[48,2048]{1,0:T(8,128)(2,1)S(1)} %get-tuple-element.15), channel_id=1, source_target_pairs={{0,6},{1,11},{2,8},{3,13},{4,10},{5,15},{6,12},{7,1},{8,14},{9,3},... | collective-permute-start | bytes 589832 | tf_op jit(solution)/shard_map/ppermute | solution.py:117
  119.5 1.6 add_convert_fusion.3
  121.1 4.1 %collective-permute-start.8 = (bf16[24,2048]{1,0:T(8,128)(2,1)}, bf16[24,2048]{1,0:T(8,128)(2,1)}, u32[]{:S(2)}, u32[]{:S(2)}) collective-permute-start(bf16[24,2048]{1,0:T(8,128)(2,1)} %add_convert_fusion.3), channel_id=1, source_target_pairs={{0,8},{2,10},{4,12},{6,14},{8,0},{10,2},{12,4},{14,6},{1,9},{3,11}... | collective-permute-start | bytes 294920 | tf_op jit(solution)/shard_map/ppermute | solution.py:25
  125.3 2.1 reduce_sum.59
  127.3 4.9 %collective-permute-done.9 = bf16[48,2048]{1,0:T(8,128)(2,1)} collective-permute-done((bf16[48,2048]{1,0:T(8,128)(2,1)S(1)}, bf16[48,2048]{1,0:T(8,128)(2,1)}, u32[]{:S(2)}, u32[]{:S(2)}) %collective-permute-start.9) | collective-permute-done | bytes 196640 | tf_op jit(solution)/shard_map/ppermute | solution.py:117
  132.2 1.2 convert_add_fusion
  133.4 0.7 dynamic-slice_convert_fusion
  134.0 1.9 collective-permute-start.12
  136.0 1.6 collective-permute-done.12
  137.6 1.2 fusion.14
  138.9 1.0 broadcast_in_dim.58
  139.9 5.7 %all-to-all-start.2 = ((bf16[8,24,2048]{2,1,0:T(8,128)(2,1)}), bf16[8,24,2048]{2,1,0:T(8,128)(2,1)S(1)}, u32[]{:S(2)}, u32[]{:S(2)}) async-start(bf16[8,24,2048]{2,1,0:T(8,128)(2,1)} %broadcast_in_dim.58), calls=%async_computation.2 | async-start | bytes 1572864 | tf_op jit(solution)/shard_map/all_to_all | solution.py:16
  145.7 23.3 %all-to-all-done.2 = bf16[8,24,2048]{2,1,0:T(8,128)(2,1)S(1)} async-done(((bf16[8,24,2048]{2,1,0:T(8,128)(2,1)}), bf16[8,24,2048]{2,1,0:T(8,128)(2,1)S(1)}, u32[]{:S(2)}, u32[]{:S(2)}) %all-to-all-start.2) | async-done | bytes 786464 | tf_op jit(solution)/shard_map/all_to_all | solution.py:16
  169.0 1.1 broadcast_in_dim.60
  170.3 6.8 %all-to-all-start.3 = ((bf16[8,256,256]{2,1,0:T(8,128)(2,1)}), bf16[8,256,256]{2,1,0:T(8,128)(2,1)S(1)}, u32[]{:S(2)}, u32[]{:S(2)}) async-start(bf16[8,256,256]{2,1,0:T(8,128)(2,1)} %broadcast_in_dim.60), calls=%async_computation.3 | async-start | bytes 2097152 | tf_op jit(solution)/shard_map/all_to_all | solution.py:16
  177.2 1.9 collective-permute-start.13
  179.1 25.7 %all-to-all-done.3 = bf16[8,256,256]{2,1,0:T(8,128)(2,1)S(1)} async-done(((bf16[8,256,256]{2,1,0:T(8,128)(2,1)}), bf16[8,256,256]{2,1,0:T(8,128)(2,1)S(1)}, u32[]{:S(2)}, u32[]{:S(2)}) %all-to-all-start.3) | async-done | bytes 1048608 | tf_op jit(solution)/shard_map/all_to_all | solution.py:16
  205.0 3.9 %collective-permute-start.14 = (f32[256]{0:T(256)S(1)}, f32[256]{0:T(256)S(1)}, u32[]{:S(2)}, u32[]{:S(2)}) collective-permute-start(f32[256]{0:T(256)S(1)} %multiply_reduce_fusion), channel_id=1, source_target_pairs={{0,128},{128,0},{256,384},{384,256},{512,640},{640,512},{768,896},... | collective-permute-start | bytes 3080 | tf_op jit(solution)/shard_map/ppermute | solution.py:29
  208.9 1.7 collective-permute-done.14
  210.6 4.7 %collective-permute-start.15 = (f32[256]{0:T(256)S(1)}, f32[256]{0:T(256)S(1)}, u32[]{:S(2)}, u32[]{:S(2)}) collective-permute-start(f32[256]{0:T(256)S(1)} %add.340), channel_id=1, source_target_pairs={{0,256},{128,384},{256,0},{384,128},{512,768},{640,896},{768,512},... | collective-permute-start | bytes 3080 | tf_op jit(solution)/shard_map/ppermute | solution.py:29
  215.6 1.4 collective-permute-done.15
  216.9 7.7 %collective-permute-start.16 = (f32[256]{0:T(256)S(1)}, f32[256]{0:T(256)S(1)}, u32[]{:S(2)}, u32[]{:S(2)}) collective-permute-start(f32[256]{0:T(256)S(1)} %add.341), channel_id=1, source_target_pairs={{0,512},{128,640},{256,768},{384,896},{512,0},{640,128},{768,256},... | collective-permute-start | bytes 3080 | tf_op jit(solution)/shard_map/ppermute | solution.py:29
  224.7 0.6 dynamic-slice_bitcast_fusion
  225.3 1.0 collective-permute-done.16
  226.3 0.6 add.342
  226.9 1.2 constant_dynamic-update-slice_fusion
  228.1 1.1 copy-done.7
  (49 shorter events, 2.3 us)
Async XLA Ops:
  0.6 86.7 %copy-start = (bf16[384,2048]{1,0:T(8,128)(2,1)S(1)}, bf16[384,2048]{1,0:T(8,128)(2,1)}, u32[]{:S(2)}) copy-start(bf16[384,2048]{1,0:T(8,128)(2,1)} %param.11) | copy-start | bytes 4718596
  0.6 38.9 %copy-start.1 = (bf16[384,2048]{1,0:T(8,128)(2,1)S(1)}, bf16[384,2048]{1,0:T(8,128)(2,1)}, u32[]{:S(2)}) copy-start(bf16[384,2048]{1,0:T(8,128)(2,1)} %param.6) | copy-start | bytes 4718596
  0.7 38.9 %copy-start.10 = (f32[2048]{0:T(1024)S(1)}, f32[2048]{0:T(1024)}, u32[]{:S(2)}) copy-start(f32[2048]{0:T(1024)} %param.7) | copy-start | bytes 24580
  2.4 31.4 %all-to-all-start = ((bf16[8,32,768]{2,1,0:T(8,128)(2,1)}), bf16[8,32,768]{2,1,0:T(8,128)(2,1)S(1)}, u32[]{:S(2)}, u32[]{:S(2)}) async-start(bf16[8,32,768]{2,1,0:T(8,128)(2,1)} %broadcast_in_dim.49), calls=%async_computation | async-start | bytes 786432 | tf_op jit(solution)/shard_map/all_to_all | solution.py:16
  33.7 12.1 %collective-permute-start = (bf16[8,32,768]{2,1,0:T(8,128)(2,1)S(1)}, bf16[8,32,768]{2,1,0:T(8,128)(2,1)}, u32[]{:S(2)}, u32[]{:S(2)}) collective-permute-start(bf16[8,32,768]{2,1,0:T(8,128)(2,1)S(1)} %all-to-all-done), channel_id=1, source_target_pairs={{0,112},{16,0},{32,16},{48,32},{64,48},{80,64},{96,80},{112,96},{1... | collective-permute-start | bytes 1179656 | tf_op jit(solution)/shard_map/ppermute | solution.py:25
  36.0 14.4 %collective-permute-start.1 = (bf16[8,32,768]{2,1,0:T(8,128)(2,1)S(1)}, bf16[8,32,768]{2,1,0:T(8,128)(2,1)}, u32[]{:S(2)}, u32[]{:S(2)}) collective-permute-start(bf16[8,32,768]{2,1,0:T(8,128)(2,1)S(1)} %all-to-all-done), channel_id=1, source_target_pairs={{0,16},{16,32},{32,48},{48,64},{64,80},{80,96},{96,112},{112,0},{1... | collective-permute-start | bytes 1179656 | tf_op jit(solution)/shard_map/ppermute | solution.py:25
  45.9 11.4 %collective-permute-start.2 = (bf16[8,32,768]{2,1,0:T(8,128)(2,1)}, bf16[8,32,768]{2,1,0:T(8,128)(2,1)S(1)}, u32[]{:S(2)}, u32[]{:S(2)}) collective-permute-start(bf16[8,32,768]{2,1,0:T(8,128)(2,1)} %collective-permute-done), channel_id=1, source_target_pairs={{0,112},{16,0},{32,16},{48,32},{64,48},{80,64},{96,80},{112,96},{1... | collective-permute-start | bytes 1179656 | tf_op jit(solution)/shard_map/ppermute | solution.py:25
  50.4 12.6 %collective-permute-start.3 = (bf16[8,32,768]{2,1,0:T(8,128)(2,1)}, bf16[8,32,768]{2,1,0:T(8,128)(2,1)S(1)}, u32[]{:S(2)}, u32[]{:S(2)}) collective-permute-start(bf16[8,32,768]{2,1,0:T(8,128)(2,1)} %collective-permute-done.1), channel_id=1, source_target_pairs={{0,16},{16,32},{32,48},{48,64},{64,80},{80,96},{96,112},{112,0},{1... | collective-permute-start | bytes 1179656 | tf_op jit(solution)/shard_map/ppermute | solution.py:25
  57.3 19.2 %collective-permute-start.4 = (bf16[8,32,768]{2,1,0:T(8,128)(2,1)S(1)}, bf16[8,32,768]{2,1,0:T(8,128)(2,1)S(1)}, u32[]{:S(2)}, u32[]{:S(2)}) collective-permute-start(bf16[8,32,768]{2,1,0:T(8,128)(2,1)S(1)} %collective-permute-done.2), channel_id=1, source_target_pairs={{0,112},{16,0},{32,16},{48,32},{64,48},{80,64},{96,80},{112,96},{1... | collective-permute-start | bytes 1179656 | tf_op jit(solution)/shard_map/ppermute | solution.py:25
  63.0 11.5 %collective-permute-start.5 = (bf16[8,32,768]{2,1,0:T(8,128)(2,1)S(1)}, bf16[8,32,768]{2,1,0:T(8,128)(2,1)S(1)}, u32[]{:S(2)}, u32[]{:S(2)}) collective-permute-start(bf16[8,32,768]{2,1,0:T(8,128)(2,1)S(1)} %collective-permute-done.3), channel_id=1, source_target_pairs={{0,16},{16,32},{32,48},{48,64},{64,80},{80,96},{96,112},{112,0},{1... | collective-permute-start | bytes 1179656 | tf_op jit(solution)/shard_map/ppermute | solution.py:25
  65.0 21.3 %copy-start.8 = (bf16[384,2048]{1,0:T(8,128)(2,1)S(1)}, bf16[384,2048]{1,0:T(8,128)(2,1)}, u32[]{:S(2)}) copy-start(bf16[384,2048]{1,0:T(8,128)(2,1)} %fusion.2) | copy-start | bytes 4718596
  74.5 10.6 %collective-permute-start.6 = (bf16[8,32,768]{2,1,0:T(8,128)(2,1)S(1)}, bf16[8,32,768]{2,1,0:T(8,128)(2,1)S(1)}, u32[]{:S(2)}, u32[]{:S(2)}) collective-permute-start(bf16[8,32,768]{2,1,0:T(8,128)(2,1)S(1)} %collective-permute-done.5), channel_id=1, source_target_pairs={{0,16},{16,32},{32,48},{48,64},{64,80},{80,96},{96,112},{112,0},{1... | collective-permute-start | bytes 1179656 | tf_op jit(solution)/shard_map/ppermute | solution.py:25
  85.1 2.2 copy-start.2
  87.3 0.9 copy-start.11
  89.3 36.0 %all-to-all-start.1 = ((bf16[8,256,256]{1,2,0:T(8,128)(2,1)}), bf16[8,256,256]{1,2,0:T(8,128)(2,1)}, u32[]{:S(2)}, u32[]{:S(2)}) async-start(bf16[8,256,256]{1,2,0:T(8,128)(2,1)} %bitcast.55), calls=%async_computation.1 | async-start | bytes 2097152 | tf_op jit(solution)/shard_map/all_to_all | solution.py:16
  93.5 2.4 %copy-start.3 = (bf16[8,8,32,768]{3,2,1,0:T(8,128)(2,1)S(1)}, bf16[8,8,32,768]{3,2,1,0:T(8,128)(2,1)}, u32[]{:S(2)}) copy-start(bf16[8,8,32,768]{3,2,1,0:T(8,128)(2,1)} %copy-done.2) | copy-start | bytes 9437188
  97.0 2.8 %copy-start.6 = (bf16[384,2048]{1,0:T(8,128)(2,1)}, bf16[384,2048]{1,0:T(8,128)(2,1)S(1)}, u32[]{:S(2)}) copy-start(bf16[384,2048]{1,0:T(8,128)(2,1)S(1)} %convolution_convert_fusion) | copy-start | bytes 4718596
  100.4 4.5 %collective-permute-start.7 = (bf16[192,2048]{1,0:T(8,128)(2,1)}, bf16[192,2048]{1,0:T(8,128)(2,1)}, u32[]{:S(2)}, u32[]{:S(2)}) collective-permute-start(bf16[192,2048]{1,0:T(8,128)(2,1)} %dynamic-slice_dynamic-update-slice_fusion.3), channel_id=1, source_target_pairs={{0,1},{1,0},{2,3},{3,2},{4,5},{5,4},{6,7},{7,6},{8,9},{9,8},{10,11... | collective-permute-start | bytes 2359304 | tf_op jit(solution)/shard_map/ppermute | solution.py:29
  107.1 20.3 %collective-permute-start.10 = (bf16[48,2048]{1,0:T(8,128)(2,1)}, bf16[48,2048]{1,0:T(8,128)(2,1)}, u32[]{:S(2)}, u32[]{:S(2)}) collective-permute-start(bf16[48,2048]{1,0:T(8,128)(2,1)} %get-tuple-element.14), channel_id=1, source_target_pairs={{0,4},{1,13},{2,6},{3,15},{4,8},{5,1},{6,10},{7,3},{8,12},{9,5},{1... | collective-permute-start | bytes 589832 | tf_op jit(solution)/shard_map/ppermute | solution.py:117
  111.4 15.9 %collective-permute-start.11 = (bf16[48,2048]{1,0:T(8,128)(2,1)S(1)}, bf16[48,2048]{1,0:T(8,128)(2,1)}, u32[]{:S(2)}, u32[]{:S(2)}) collective-permute-start(bf16[48,2048]{1,0:T(8,128)(2,1)S(1)} %get-tuple-element.13), channel_id=1, source_target_pairs={{0,2},{1,15},{2,4},{3,1},{4,6},{5,3},{6,8},{7,5},{8,10},{9,7},{10,... | collective-permute-start | bytes 589832 | tf_op jit(solution)/shard_map/ppermute | solution.py:117
  114.8 17.4 %collective-permute-start.9 = (bf16[48,2048]{1,0:T(8,128)(2,1)S(1)}, bf16[48,2048]{1,0:T(8,128)(2,1)}, u32[]{:S(2)}, u32[]{:S(2)}) collective-permute-start(bf16[48,2048]{1,0:T(8,128)(2,1)S(1)} %get-tuple-element.15), channel_id=1, source_target_pairs={{0,6},{1,11},{2,8},{3,13},{4,10},{5,15},{6,12},{7,1},{8,14},{9,3},... | collective-permute-start | bytes 589832 | tf_op jit(solution)/shard_map/ppermute | solution.py:117
  121.1 14.9 %collective-permute-start.8 = (bf16[24,2048]{1,0:T(8,128)(2,1)}, bf16[24,2048]{1,0:T(8,128)(2,1)}, u32[]{:S(2)}, u32[]{:S(2)}) collective-permute-start(bf16[24,2048]{1,0:T(8,128)(2,1)} %add_convert_fusion.3), channel_id=1, source_target_pairs={{0,8},{2,10},{4,12},{6,14},{8,0},{10,2},{12,4},{14,6},{1,9},{3,11}... | collective-permute-start | bytes 294920 | tf_op jit(solution)/shard_map/ppermute | solution.py:25
  134.0 3.5 %collective-permute-start.12 = (bf16[24,2048]{1,0:T(8,128)(2,1)}, bf16[24,2048]{1,0:T(8,128)(2,1)}, u32[]{:S(2)}, u32[]{:S(2)}) collective-permute-start(bf16[24,2048]{1,0:T(8,128)(2,1)} %dynamic-slice_convert_fusion), channel_id=1, source_target_pairs={{0,1},{1,0},{2,3},{3,2},{4,5},{5,4},{6,7},{7,6},{8,9},{9,8},{10,11... | collective-permute-start | bytes 294920 | tf_op jit(solution)/shard_map/ppermute | solution.py:29
  138.8 6.8 %copy-start.9 = (bf16[256,256]{0,1:T(8,128)(2,1)S(1)}, bf16[256,256]{0,1:T(8,128)(2,1)}, u32[]{:S(2)}) copy-start(bf16[256,256]{0,1:T(8,128)(2,1)} %reduce_sum.59) | copy-start | bytes 393220
  139.9 29.1 %all-to-all-start.2 = ((bf16[8,24,2048]{2,1,0:T(8,128)(2,1)}), bf16[8,24,2048]{2,1,0:T(8,128)(2,1)S(1)}, u32[]{:S(2)}, u32[]{:S(2)}) async-start(bf16[8,24,2048]{2,1,0:T(8,128)(2,1)} %broadcast_in_dim.58), calls=%async_computation.2 | async-start | bytes 1572864 | tf_op jit(solution)/shard_map/all_to_all | solution.py:16
  169.0 1.3 copy-start.4
  170.3 34.4 %all-to-all-start.3 = ((bf16[8,256,256]{2,1,0:T(8,128)(2,1)}), bf16[8,256,256]{2,1,0:T(8,128)(2,1)S(1)}, u32[]{:S(2)}, u32[]{:S(2)}) async-start(bf16[8,256,256]{2,1,0:T(8,128)(2,1)} %broadcast_in_dim.60), calls=%async_computation.3 | async-start | bytes 2097152 | tf_op jit(solution)/shard_map/all_to_all | solution.py:16
  177.2 49.7 %collective-permute-start.13 = (bf16[8,1,24,2048]{3,2,1,0:T(8,128)(2,1)}, bf16[8,1,24,2048]{3,2,1,0:T(8,128)(2,1)}, u32[]{:S(2)}, u32[]{:S(2)}) collective-permute-start(bf16[8,1,24,2048]{3,2,1,0:T(8,128)(2,1)} %bitcast.56), channel_id=1, source_target_pairs={{0,1},{1,0},{2,3},{3,2},{4,5},{5,4},{6,7},{7,6},{8,9},{9,8},{10,11... | collective-permute-start | bytes 2359304 | tf_op jit(solution)/shard_map/ppermute | solution.py:29
  204.9 10.6 %copy-start.5 = (bf16[8,24,2048]{2,1,0:T(8,128)(2,1)S(1)}, bf16[8,24,2048]{2,1,0:T(8,128)(2,1)}, u32[]{:S(2)}) copy-start(bf16[8,24,2048]{2,1,0:T(8,128)(2,1)} %copy-done.4) | copy-start | bytes 2359300
  205.0 5.6 %collective-permute-start.14 = (f32[256]{0:T(256)S(1)}, f32[256]{0:T(256)S(1)}, u32[]{:S(2)}, u32[]{:S(2)}) collective-permute-start(f32[256]{0:T(256)S(1)} %multiply_reduce_fusion), channel_id=1, source_target_pairs={{0,128},{128,0},{256,384},{384,256},{512,640},{640,512},{768,896},... | collective-permute-start | bytes 3080 | tf_op jit(solution)/shard_map/ppermute | solution.py:29
  210.6 6.4 %collective-permute-start.15 = (f32[256]{0:T(256)S(1)}, f32[256]{0:T(256)S(1)}, u32[]{:S(2)}, u32[]{:S(2)}) collective-permute-start(f32[256]{0:T(256)S(1)} %add.340), channel_id=1, source_target_pairs={{0,256},{128,384},{256,0},{384,128},{512,768},{640,896},{768,512},... | collective-permute-start | bytes 3080 | tf_op jit(solution)/shard_map/ppermute | solution.py:29
  216.9 9.4 %collective-permute-start.16 = (f32[256]{0:T(256)S(1)}, f32[256]{0:T(256)S(1)}, u32[]{:S(2)}, u32[]{:S(2)}) collective-permute-start(f32[256]{0:T(256)S(1)} %add.341), channel_id=1, source_target_pairs={{0,512},{128,640},{256,768},{384,896},{512,0},{640,128},{768,256},... | collective-permute-start | bytes 3080 | tf_op jit(solution)/shard_map/ppermute | solution.py:29
  228.1 1.1 copy-start.7
